TPU v7x, 32 devices: a whole 2x2x4 slice. The times are simulated.
32 devices in a mesh: kv: 8 (over z, x), tp: 4 (over y, core).
Axes of the slice: x: 2, y: 2, z: 4, core: 2. Of those that a mesh axis runs over, the one named last changes fastest.
Arguments:
- activations: bfloat16 [384, 2048], P(None, ('kv', 'tp')), may hold values from -6 to 6
- latent_cache: bfloat16 [24, 16384, 288], P(None, 'kv'), may hold values from -6 to 6
- lengths: int32 [24], replicated, may hold values from 4096 to 16352, as said below
- accepted: int32 [24], replicated, may hold values from 0 to 16
- parents: int32 [24, 16], replicated, may hold values from -1 to 14, as said below
- w_query_down: bfloat16 [2048, 512], P(('kv', 'tp')), may hold values from -0.125 to 0.125
- w_key_down: bfloat16 [2048, 288], P(('kv', 'tp')), may hold values from -0.125 to 0.125
- gain_input: bfloat16 [2048], P(('kv', 'tp')), may hold values from 0.099609375 to 1.8984375
- gain_query: bfloat16 [512], replicated, may hold values from 0.099609375 to 1.8984375
- gain_key: bfloat16 [256], replicated, may hold values from 0.099609375 to 1.8984375
- w_query: bfloat16 [512, 16, 288], P(None, 'tp'), as said below
- w_value: bfloat16 [16, 256, 64], replicated, may hold values from -0.375 to 0.375
- w_out: bfloat16 [1024, 2048], P('tp', 'kv'), may hold values from -1 to 1, as said below
- gain_output: bfloat16 [2048], P('kv'), may hold values from 0.099609375 to 1.8984375
Outputs:
- mixed: bfloat16 [384, 2048], P(None, 'kv')
- new_cache: bfloat16 [24, 16384, 288], P(None, 'kv')
Inputs may be any that keep to these rules, and one draw needn't show every extreme that they name: One sequence has lengths exactly 16352 and another exactly 4096; which ones varies. accepted is between 0 and 16, so the proposals' positions lie below 16384. `parents`: the parent of proposal i is -1 or a proposal with a smaller index; proposal 0 has parent -1; the proposals of exactly one sequence (which one varies) form a single chain; the other sequences' proposals form general trees. `w_query`: entries are normal with standard deviation (1536)^(-1/2) cut at six standard deviations; in the hidden draw the heads whose index is a multiple of 4 are 48 times larger. `w_out`: entries of order (1024)^(-1/2).
All inputs are finite; a program needn't handle non-finite values.
Results may differ from a plain program's by a relative error of at most 0.0096.
The roundings to bfloat16 on the way count: a program that leaves them out, or rounds other values in their place, can miss the bound.
Values may be sent and summed in bfloat16 or wider, within the bound.
A program may use at most 192 MiB of HBM per device.

v0:
```python
import functools

import jax
import jax.numpy as jnp
from jax import lax
from jax.experimental import pallas as pl
from jax.experimental.pallas import tpu as pltpu
from jax.sharding import PartitionSpec as P

NOPE_DIM = 64
LANES = 128

epsilon = 1e-06
rope_base = 10000.0
score_after_mask = -1e30
MESH = pl.DeviceIdType.MESH
HIGHEST = lax.Precision.HIGHEST
VMEM = pl.BlockSpec(memory_space=pltpu.VMEM)


def ancestry(parents):
    seq_count, prop_count = parents.shape
    slot_ids = jnp.arange(prop_count, dtype=jnp.int32)
    parent_links = (parents[:, :, None] == slot_ids[None, None, :]).astype(jnp.bfloat16)
    identity = jnp.broadcast_to(jnp.eye(prop_count, dtype=jnp.bfloat16), parent_links.shape)
    reached = jnp.minimum(identity + parent_links, 1.0)
    for repeat in range((prop_count - 1).bit_length()):
        reached = jnp.minimum(
            jnp.einsum("sij,sjk->sik", reached, reached, preferred_element_type=jnp.float32), 1.0
        ).astype(jnp.bfloat16)
    depths = (jnp.sum(reached.astype(jnp.float32), axis=-1) - 1.0).astype(jnp.int32)
    return (reached, depths)


def dot(a, b, precision=None):
    return jnp.dot(a, b, preferred_element_type=jnp.float32, precision=precision)


def dot_nt(a, b, precision=None):
    return lax.dot_general(
        a, b, (((1,), (1,)), ((), ())), preferred_element_type=jnp.float32, precision=precision
    )


def remote(src, dst, send_sem, recv_sem, device_id):
    return pltpu.make_async_remote_copy(
        src_ref=src,
        dst_ref=dst,
        send_sem=send_sem,
        recv_sem=recv_sem,
        device_id=device_id,
        device_id_type=MESH,
    )


def root_mean(values, count):
    return lax.rsqrt(jnp.sum(values * values, axis=-1, keepdims=True) / count + epsilon)


def compress_kernel(
    n_kv, n_tp, width, q_rank, kv_rank, turn_dim,
    x_ref, w_ref, cos_ref, sin_ref, gain_q_ref, gain_k_ref, out_ref,
    got_x, got_w, part, got_part, all_rows,
    send_x, recv_x, send_w, recv_w, send_p, recv_p, send_a, send_y, send_b, recv_a,
):
    me_k, me_t = lax.axis_index("kv"), lax.axis_index("tp")
    barrier = pltpu.get_barrier_semaphore()
    for dk in range(n_kv):
        for dt in range(n_tp):
            if dk or dt:
                pl.semaphore_signal(
                    barrier,
                    inc=1,
                    device_id={"kv": lax.rem(me_k + dk, n_kv), "tp": lax.rem(me_t + dt, n_tp)},
                    device_id_type=MESH,
                )
    pl.semaphore_wait(barrier, n_kv * n_tp - 1)

    sends = []
    features = w_ref.shape[0]
    for d in range(1, n_tp):
        peer = lax.rem(me_t + d, n_tp)
        for src, dst, ss, rs in (
            (x_ref.at[peer], got_x.at[me_t], send_x.at[d], recv_x.at[me_t]),
            (w_ref, got_w.at[me_t], send_w.at[d], recv_w.at[me_t]),
        ):
            copy = remote(src, dst, ss, rs, {"tp": peer})
            copy.start()
            sends.append(copy)

    def term(x, w):
        raw = x[:, features:].astype(jnp.float32)
        return dot(x[:, :features], w), jnp.sum(raw * raw, axis=-1, keepdims=True)

    total, squares = term(x_ref[me_t], w_ref[...])
    for d in range(1, n_tp):
        peer = lax.rem(me_t + d, n_tp)
        remote(x_ref.at[peer], got_x.at[peer], send_x.at[d], recv_x.at[peer], {"tp": peer}).wait_recv()
        remote(w_ref, got_w.at[peer], send_w.at[d], recv_w.at[peer], {"tp": peer}).wait_recv()
        more, more_squares = term(got_x[peer], got_w[peer])
        total, squares = total + more, squares + more_squares
    lane = lax.broadcasted_iota(jnp.int32, total.shape, 1)
    total = jnp.where(lane == width - 1, squares, total)
    each = part.shape[1]
    for j in range(n_kv):
        part[j] = total[j * each : (j + 1) * each]

    for d in range(1, n_kv):
        peer = lax.rem(me_k + d, n_kv)
        copy = remote(part.at[peer], got_part.at[me_k], send_p.at[d], recv_p.at[me_k], {"kv": peer})
        copy.start()
        sends.append(copy)
    summed = part[me_k]
    for d in range(1, n_kv):
        peer = lax.rem(me_k + d, n_kv)
        remote(
            part.at[peer], got_part.at[peer], send_p.at[d], recv_p.at[peer], {"kv": peer}
        ).wait_recv()
        summed = summed + got_part[peer]
    model = n_kv * n_tp * features
    inverse = lax.rsqrt(summed[:, width - 1 : width] / model + epsilon)
    query = summed[:, :q_rank] * inverse
    query = query * root_mean(query, q_rank) * gain_q_ref[...]
    latent = summed[:, q_rank : q_rank + kv_rank] * inverse
    latent = latent * root_mean(latent, kv_rank) * gain_k_ref[...]
    turn = summed[:, q_rank + kv_rank :] * inverse
    tail = turn.shape[1]
    swapped = pltpu.roll(turn, tail - turn_dim, 1)
    turned = turn * cos_ref[...] + swapped * sin_ref[...]
    mine = me_t * n_kv + me_k
    all_rows[mine, :, :q_rank] = query.astype(jnp.bfloat16)
    all_rows[mine, :, q_rank : q_rank + kv_rank] = latent.astype(jnp.bfloat16)
    all_rows[mine, :, q_rank + kv_rank :] = turned.astype(jnp.bfloat16)

    sibling = me_t + 1 - 2 * lax.rem(me_t, 2)
    def send(block, sem, device_id):
        copy = remote(all_rows.at[block], all_rows.at[block], sem, recv_a.at[block], device_id)
        copy.start()
        sends.append(copy)

    def landed(block):
        remote(
            all_rows.at[block], all_rows.at[block], send_a.at[0], recv_a.at[block], {"tp": sibling}
        ).wait_recv()

    for dk in range(1, n_kv):
        send(mine, send_a.at[dk], {"kv": lax.rem(me_k + dk, n_kv)})
    for dk in range(n_kv):
        block = me_t * n_kv + lax.rem(me_k + dk, n_kv)
        if dk:
            landed(block)
        for dy in range(1, n_tp // 2):
            send(block, send_y.at[dy * n_kv + dk], {"tp": lax.rem(me_t + 2 * dy, n_tp)})
        send(block, send_b.at[dk], {"tp": sibling})
    for dy in range(1, n_tp // 2):
        for dk in range(n_kv):
            block = lax.rem(me_t + 2 * dy, n_tp) * n_kv + lax.rem(me_k + dk, n_kv)
            landed(block)
            send(block, send_b.at[dy * n_kv + dk], {"tp": sibling})
    for dy in range(n_tp // 2):
        for dk in range(n_kv):
            block = lax.rem(sibling + 2 * dy, n_tp) * n_kv + lax.rem(me_k + dk, n_kv)
            landed(block)
    out_ref[...] = all_rows[...]
    for copy in sends:
        copy.wait_send()


def attend_kernel(
    group, rel_ref, low_ref, wq_ref, cos_ref, sin_ref, reached_ref, fresh_ref, cache_ref,
    out_ref, part_ref, stats_ref, q_main, q_turn, bias,
):
    heads, whole, _ = wq_ref.shape
    turn_dim = q_turn.shape[-1]
    rank = whole - turn_dim
    half = turn_dim // 2
    props = reached_ref.shape[-1]
    seqs = q_main.shape[0]
    span = cache_ref.shape[-1]
    step = pl.program_id(0)
    scale = (NOPE_DIM + turn_dim) ** (-0.5)

    @pl.when(step == 0)
    def _():
        low = low_ref[...]
        for h in range(heads):
            main = dot_nt(low, wq_ref[h, :rank, :])
            front, back = wq_ref[h, rank : rank + half, :], wq_ref[h, rank + half :, :]
            turn = dot_nt(low, jnp.concatenate([front, back], axis=0))
            swapped = dot_nt(low, jnp.concatenate([back, front], axis=0))
            turned = turn * cos_ref[...] + swapped * sin_ref[...]
            rows = slice(h * props, (h + 1) * props)
            q_main[:, rows, :] = main.astype(jnp.bfloat16).reshape(seqs, props, rank)
            q_turn[:, rows, :] = turned.astype(jnp.bfloat16).reshape(seqs, props, turn_dim)

    for g in range(group):
        s = step * group + g
        rel = rel_ref[s]
        out_ref[g] = cache_ref[g]
        past = lax.broadcasted_iota(jnp.int32, (props, span), 1) < rel
        bias[g] = jnp.where(past, 0.0, score_after_mask)
        first = lax.shift_right_arithmetic(rel, 7)
        for more in range(2):
            chunk = first + more

            @pl.when((chunk >= 0) & (chunk < span // LANES))
            def _():
                start = pl.multiple_of(chunk * LANES, LANES)
                slot = start - rel + lax.broadcasted_iota(jnp.int32, (props, LANES), 1)
                onehot = slot == lax.broadcasted_iota(jnp.int32, (props, LANES), 0)
                onehot = onehot.astype(jnp.float32).astype(jnp.bfloat16)
                seen = (slot < 0) | (dot(reached_ref[g], onehot) > 0.5)
                bias[g, :, pl.ds(start, LANES)] = jnp.where(seen, 0.0, score_after_mask)
                placed = lax.dot_general(
                    fresh_ref[g], onehot, (((0,), (0,)), ((), ())),
                    preferred_element_type=jnp.float32,
                )
                slots = start - rel + lax.broadcasted_iota(jnp.int32, placed.shape, 1)
                old = out_ref[g, :, pl.ds(start, LANES)].astype(jnp.float32)
                new = jnp.where((slots >= 0) & (slots < props), placed, old)
                out_ref[g, :, pl.ds(start, LANES)] = new.astype(jnp.bfloat16)

    for g in range(group):
        s = step * group + g
        scores = dot(q_main[s], out_ref[g, :rank, :]) + dot(q_turn[s], out_ref[g, rank:, :])
        masked = scores.reshape(heads, props, span) * scale + bias[g][None]
        top = jnp.max(masked, axis=-1, keepdims=True)
        weights = jnp.exp(masked - jnp.maximum(top, -1e29))
        totals = jnp.sum(weights, axis=-1, keepdims=True)
        prob = weights.astype(jnp.bfloat16).reshape(heads * props, span)
        weighted = dot_nt(prob, out_ref[g, :rank, :]).reshape(heads, props, rank)
        part = (weighted / jnp.maximum(totals, 1.0)).astype(jnp.bfloat16)
        lane = lax.broadcasted_iota(jnp.int32, (props, LANES), 1)
        stats = jnp.zeros((props, LANES), jnp.float32)
        rows = slice(g * props, (g + 1) * props)
        for h in range(heads):
            part_ref[h, rows, :] = part[h]
            stats = jnp.where(lane == h, top[h], stats)
            stats = jnp.where(lane == heads + h, totals[h], stats)
        stats_ref[rows, :] = stats


def project_kernel(
    n_kv, n_tp,
    part_ref, stats_ref, wv_ref, w_out_ref, gain_ref, out_ref,
    vals, stat, got_vals, got_stat, attended, raw, got_raw, sums, result,
    send_v, recv_v, send_s, recv_s, send_a, recv_a, send_r, recv_r, send_q, recv_q, send_o, recv_o,
):
    me_k, me_t = lax.axis_index("kv"), lax.axis_index("tp")
    heads, _, _ = part_ref.shape
    v_dim = wv_ref.shape[1]
    kv_peers = [lax.rem(me_k + d, n_kv) for d in range(n_kv)]
    tp_peers = [lax.rem(me_t + d, n_tp) for d in range(n_tp)]
    barrier = pltpu.get_barrier_semaphore()
    for peer in kv_peers[1:]:
        pl.semaphore_signal(barrier, inc=1, device_id={"kv": peer}, device_id_type=MESH)
    for peer in tp_peers[1:]:
        pl.semaphore_signal(barrier, inc=1, device_id={"tp": peer}, device_id_type=MESH)
    sends = []

    each = vals.shape[1]
    line = lax.broadcasted_iota(jnp.int32, (16, LANES), 0)
    lane = lax.broadcasted_iota(jnp.int32, (16, LANES), 1)
    tops = (line < heads) & (lane == line)
    counts = (line >= 8) & (line < 8 + heads) & (lane == line - 8 + heads)
    pick = jnp.where(tops | counts, 1.0, 0.0)
    values = jnp.concatenate([dot_nt(part_ref[h], wv_ref[h]) for h in range(heads)], axis=1)
    for j in range(n_kv):
        vals[j] = values[j * each : (j + 1) * each].astype(jnp.bfloat16)
        stat[j] = dot_nt(pick, stats_ref[j * each : (j + 1) * each, :], HIGHEST)
    pl.semaphore_wait(barrier, n_kv + n_tp - 2)

    def exchange(axis, peers, src_of, dst, own, send_sem, recv_sem):
        for d in range(1, len(peers)):
            copy = remote(
                src_of(peers[d]), dst.at[own], send_sem.at[d], recv_sem.at[own], {axis: peers[d]}
            )
            copy.start()
            sends.append(copy)

    def arrived(axis, peers, d, src_of, dst, send_sem, recv_sem):
        remote(
            src_of(peers[d]), dst.at[peers[d]], send_sem.at[d], recv_sem.at[peers[d]],
            {axis: peers[d]},
        ).wait_recv()

    exchange("kv", kv_peers, lambda p: stat.at[p], got_stat, me_k, send_s, recv_s)
    exchange("kv", kv_peers, lambda p: vals.at[p], got_vals, me_k, send_v, recv_v)
    for d in range(1, n_kv):
        arrived("kv", kv_peers, d, lambda p: stat.at[p], got_stat, send_s, recv_s)
    all_stats = [stat[me_k]] + [got_stat[p] for p in kv_peers[1:]]
    largest = all_stats[0][:8]
    for one in all_stats[1:]:
        largest = jnp.maximum(largest, one[:8])
    shares = jnp.concatenate([one[8:] * jnp.exp(one[:8] - largest) for one in all_stats], axis=0)
    turn_eye = lax.broadcasted_iota(jnp.int32, (each, each), 0) == lax.broadcasted_iota(
        jnp.int32, (each, each), 1
    )
    shares = dot_nt(turn_eye.astype(jnp.float32), shares, HIGHEST)
    wide = lax.broadcasted_iota(jnp.int32, (each, heads * v_dim), 1)

    def spread(d):
        out = shares[:, 8 * d : 8 * d + 1]
        for h in range(1, heads):
            out = jnp.where(wide >= h * v_dim, shares[:, 8 * d + h : 8 * d + h + 1], out)
        return jnp.broadcast_to(out, wide.shape)

    summed = None
    for d in range(n_kv):
        share = spread(d)
        if d:
            arrived("kv", kv_peers, d, lambda p: vals.at[p], got_vals, send_v, recv_v)
        block = got_vals[kv_peers[d]] if d else vals[me_k]
        term = share * block.astype(jnp.float32)
        summed = term if summed is None else summed + term
        weight = share if d == 0 else weight + share
    attended[me_k] = (summed / weight).astype(jnp.bfloat16)
    exchange("kv", kv_peers, lambda p: attended.at[me_k], attended, me_k, send_a, recv_a)
    for d in range(1, n_kv):
        arrived("kv", kv_peers, d, lambda p: attended.at[p], attended, send_a, recv_a)

    lines = jnp.concatenate([attended[j].astype(jnp.float32) for j in range(n_kv)], axis=0)
    lines = dot(lines.astype(jnp.bfloat16), w_out_ref[...])
    share_rows = raw.shape[1]
    for t in range(n_tp):
        raw[t] = lines[t * share_rows : (t + 1) * share_rows]
    exchange("tp", tp_peers, lambda p: raw.at[p], got_raw, me_t, send_r, recv_r)
    mixed = raw[me_t]
    for d in range(1, n_tp):
        arrived("tp", tp_peers, d, lambda p: raw.at[p], got_raw, send_r, recv_r)
        mixed = mixed + got_raw[tp_peers[d]]
    cols = mixed.shape[1]
    sums[me_k] = dot_nt(jnp.ones((8, cols), jnp.float32), mixed * mixed, HIGHEST)
    exchange("kv", kv_peers, lambda p: sums.at[me_k], sums, me_k, send_q, recv_q)
    for d in range(1, n_kv):
        arrived("kv", kv_peers, d, lambda p: sums.at[p], sums, send_q, recv_q)
    square = sums[0]
    for j in range(1, n_kv):
        square = square + sums[j]
    norm = lax.rsqrt(square / (cols * n_kv) + epsilon)
    eye = lax.broadcasted_iota(jnp.int32, (share_rows, share_rows), 0) == lax.broadcasted_iota(
        jnp.int32, (share_rows, share_rows), 1
    )
    column = dot_nt(eye.astype(jnp.float32), norm, HIGHEST)
    result[me_t] = (mixed * column[:, 0:1] * gain_ref[...]).astype(jnp.bfloat16)
    exchange("tp", tp_peers, lambda p: result.at[me_t], result, me_t, send_o, recv_o)
    for d in range(1, n_tp):
        arrived("tp", tp_peers, d, lambda p: result.at[p], result, send_o, recv_o)
    out_ref[...] = result[...]
    for copy in sends:
        copy.wait_send()


def up(value, to):
    return -(-value // to) * to


def local(
    n_kv,
    n_tp,
    activations,
    latent_cache,
    lengths,
    accepted,
    parents,
    w_query_down,
    w_key_down,
    gain_input,
    gain_query,
    gain_key,
    w_query,
    w_value,
    w_out,
    gain_output,
):
    bf16, f32 = jnp.bfloat16, jnp.float32
    seqs, props = parents.shape
    rows, features = activations.shape
    heads = w_query.shape[1]
    q_rank, kv_rank = gain_query.shape[0], gain_key.shape[0]
    whole = latent_cache.shape[-1]
    turn_dim = whole - kv_rank
    half = turn_dim // 2
    span = latent_cache.shape[1]
    v_dim = w_value.shape[-1]
    cols = w_out.shape[1]
    n_dev = n_kv * n_tp
    me_k, me_t = lax.axis_index("kv"), lax.axis_index("tp")

    reached, depths = ancestry(parents)
    filled = lengths + accepted
    places = (filled[:, None] + depths).reshape(-1)
    frequency = rope_base ** (-jnp.arange(half, dtype=f32) / half)
    angles = places.astype(f32)[:, None] * frequency[None, :]
    cosine, sine = jnp.cos(angles), jnp.sin(angles)
    cosine = jnp.concatenate([cosine, cosine], axis=1)
    sine = jnp.concatenate([-sine, sine], axis=1)

    few = rows // n_dev
    each = up(few, 16)
    tail = up(2 * turn_dim + 1, LANES)
    width = q_rank + kv_rank + tail

    def own_rows(table):
        mine = lax.dynamic_slice_in_dim(table, (me_t * n_kv + me_k) * few, few, 0)
        return jnp.pad(mine, ((0, each - few), (0, tail - turn_dim)))

    scaled = (activations.astype(f32) * gain_input.astype(f32)).astype(bf16)
    x = jnp.concatenate([scaled, activations], axis=1).reshape(n_dev, few, 2 * features)
    x = jnp.pad(x, ((0, 0), (0, each - few), (0, 0))).reshape(n_tp, n_kv * each, 2 * features)
    w = jnp.concatenate(
        [
            w_query_down,
            w_key_down,
            w_key_down[:, kv_rank + half :],
            w_key_down[:, kv_rank : kv_rank + half],
            jnp.zeros((features, tail - 2 * turn_dim), bf16),
        ],
        axis=1,
    )
    dma = pltpu.SemaphoreType.DMA
    gathered = pl.pallas_call(
        functools.partial(compress_kernel, n_kv, n_tp, width, q_rank, kv_rank, turn_dim),
        name="compress",
        out_shape=jax.ShapeDtypeStruct((n_dev, each, width), bf16),
        in_specs=[VMEM] * 6,
        out_specs=VMEM,
        scratch_shapes=[
            pltpu.VMEM((n_tp, n_kv * each, 2 * features), bf16),
            pltpu.VMEM((n_tp, features, width), bf16),
            pltpu.VMEM((n_kv, each, width), f32),
            pltpu.VMEM((n_kv, each, width), f32),
            pltpu.VMEM((n_dev, each, width), bf16),
            dma((n_tp,)), dma((n_tp,)), dma((n_tp,)), dma((n_tp,)),
            dma((n_kv,)), dma((n_kv,)),
            dma((n_kv,)), dma((n_dev,)), dma((n_dev,)), dma((n_dev,)),
        ],
        compiler_params=pltpu.CompilerParams(
            collective_id=0, has_side_effects=True, vmem_limit_bytes=32 * 1024 * 1024
        ),
    )(
        x, w, own_rows(cosine), own_rows(sine),
        gain_query.astype(f32)[None], gain_key.astype(f32)[None],
    )
    gathered = gathered[:, :few].reshape(rows, width)
    query_low = gathered[:, :q_rank]
    fresh = gathered[:, q_rank : q_rank + whole].reshape(seqs, props, whole)

    group = next(g for g in (3, 2, 1) if seqs % g == 0)
    fixed = lambda *shape: pl.BlockSpec(shape, lambda i, rel: (0,) * len(shape))
    updated, part, stats = pl.pallas_call(
        functools.partial(attend_kernel, group),
        name="attend",
        out_shape=(
            jax.ShapeDtypeStruct((seqs, whole, span), bf16),
            jax.ShapeDtypeStruct((heads, rows, kv_rank), bf16),
            jax.ShapeDtypeStruct((rows, LANES), f32),
        ),
        grid_spec=pltpu.PrefetchScalarGridSpec(
            num_scalar_prefetch=1,
            grid=(seqs // group,),
            in_specs=[
                fixed(rows, q_rank),
                fixed(heads, whole, q_rank),
                fixed(rows, turn_dim),
                fixed(rows, turn_dim),
                pl.BlockSpec((group, props, props), lambda i, rel: (i, 0, 0)),
                pl.BlockSpec((group, props, whole), lambda i, rel: (i, 0, 0)),
                pl.BlockSpec((group, whole, span), lambda i, rel: (i, 0, 0)),
            ],
            out_specs=[
                pl.BlockSpec((group, whole, span), lambda i, rel: (i, 0, 0)),
                pl.BlockSpec((heads, group * props, kv_rank), lambda i, rel: (0, i, 0)),
                pl.BlockSpec((group * props, LANES), lambda i, rel: (i, 0)),
            ],
            scratch_shapes=[
                pltpu.VMEM((seqs, heads * props, kv_rank), bf16),
                pltpu.VMEM((seqs, heads * props, turn_dim), bf16),
                pltpu.VMEM((group, props, span), f32),
            ],
        ),
        compiler_params=pltpu.CompilerParams(vmem_limit_bytes=48 * 1024 * 1024),
    )(
        filled - me_k * span,
        query_low,
        w_query.transpose(1, 2, 0),
        cosine,
        sine,
        reached,
        fresh,
        latent_cache.transpose(0, 2, 1),
    )

    wv = lax.dynamic_slice_in_dim(w_value.transpose(0, 2, 1), me_t * heads, heads, 0)
    per_kv, per_tp = rows // n_kv, rows // n_tp
    mixed = pl.pallas_call(
        functools.partial(project_kernel, n_kv, n_tp),
        name="project",
        out_shape=jax.ShapeDtypeStruct((n_tp, per_tp, cols), bf16),
        in_specs=[VMEM] * 5,
        out_specs=VMEM,
        scratch_shapes=[
            pltpu.VMEM((n_kv, per_kv, heads * v_dim), bf16),
            pltpu.VMEM((n_kv, 16, per_kv), f32),
            pltpu.VMEM((n_kv, per_kv, heads * v_dim), bf16),
            pltpu.VMEM((n_kv, 16, per_kv), f32),
            pltpu.VMEM((n_kv, per_kv, heads * v_dim), bf16),
            pltpu.VMEM((n_tp, per_tp, cols), f32),
            pltpu.VMEM((n_tp, per_tp, cols), f32),
            pltpu.VMEM((n_kv, 8, per_tp), f32),
            pltpu.VMEM((n_tp, per_tp, cols), bf16),
            dma((n_kv,)), dma((n_kv,)), dma((n_kv,)), dma((n_kv,)), dma((n_kv,)), dma((n_kv,)),
            dma((n_tp,)), dma((n_tp,)), dma((n_kv,)), dma((n_kv,)), dma((n_tp,)), dma((n_tp,)),
        ],
        compiler_params=pltpu.CompilerParams(
            collective_id=1, has_side_effects=True, vmem_limit_bytes=32 * 1024 * 1024
        ),
    )(part, stats, wv, w_out, gain_output.astype(f32)[None])
    return (mixed.reshape(rows, cols), updated.transpose(0, 2, 1))


def solution(mesh):
    in_specs = (
        P(None, ("kv", "tp")),
        P(None, "kv", None),
        P(),
        P(),
        P(),
        P(("kv", "tp"), None),
        P(("kv", "tp"), None),
        P(("kv", "tp")),
        P(),
        P(),
        P(None, "tp", None),
        P(),
        P("tp", "kv"),
        P("kv"),
    )
    out_specs = (P(None, "kv"), P(None, "kv", None))
    body = functools.partial(local, mesh.shape["kv"], mesh.shape["tp"])
    return jax.shard_map(body, mesh=mesh, in_specs=in_specs, out_specs=out_specs, check_vma=False)
```

profile of v0, /device:TPU:0, one launch (start us, length us, event | category | flops | bytes accessed | tf_op | source)
XLA Modules:
  0.0 108.3 jit_solution(4358962578927153205)
XLA Ops:
  0.6 0.0 copy-start
  0.6 0.0 copy-start.3
  0.7 0.0 copy-start.2
  0.7 0.7 broadcast_subtract_fusion
  1.4 0.8 copy.25
  2.2 0.5 fusion.1
  2.7 0.4 convert_reduce_fusion
  3.2 0.1 add_convert_fusion
  3.2 0.1 convert_element_type.69
  3.3 0.2 fusion.18
  3.5 0.1 copy.28.cos_ref
  3.7 0.1 copy.29.sin_ref
  3.9 0.9 fusion.23
  4.7 0.9 concatenate.13.w_ref
  5.7 0.7 convert_element_type.58
  6.3 0.9 multiply_convert_fusion
  7.2 0.8 pad_maximum_fusion
  8.0 0.1 copy.24
  8.2 0.7 broadcast_in_dim.35
  8.9 0.7 broadcast_in_dim.36
  9.6 37.2 %compress.1 = bf16[32,16,896]{2,1,0:T(8,128)(2,1)S(1)} custom-call(bf16[4,128,128]{2,1,0:T(8,128)(2,1)S(1)} %bitcast.18, bf16[64,896]{1,0:T(8,128)(2,1)S(1)} %concatenate.13.w_ref, f32[16,128]{1,0:T(8,128)S(1)} %pad.12.cos_ref, f32[16,128]{1,0:T(8,128)S(1)} %pad.13.sin_ref, f32[1,512]{1,0:T(1,128)S(1)} %bitcast.19, f32[1,256]{1,0:T(1,128)S(1)} %bitcast.21), custom_call_target="tpu_custom_call" | custom-call | tf_op jit(solution)/shard_map/compress/pallas_call | solution.py:422
  46.8 0.2 reshape.50
  47.1 0.0 copy-start.1
  47.1 1.3 %copy-done.1 = bf16[512,4,288]{0,2,1:T(8,128)(2,1)S(1)} copy-done((bf16[512,4,288]{0,2,1:T(8,128)(2,1)S(1)}, bf16[512,4,288]{0,2,1:T(8,128)(2,1)}, u32[]{:S(2)}) %copy-start.1) | copy-done | bytes 1179672
  48.3 26.1 %attend.1 = (bf16[24,288,2048]{2,1,0:T(8,128)(2,1)}, bf16[4,384,256]{2,1,0:T(8,128)(2,1)S(1)}, f32[384,128]{1,0:T(8,128)S(1)}) custom-call(s32[24]{0:T(128)S(1)} %get-tuple-element.8.rel_ref, bf16[384,512]{1,0:T(8,128)(2,1)S(1)} %slice.20.low_ref, bf16[4,288,512]{2,1,0:T(8,128)(2,1)S(1)} %bitcast.15, f32[384,32]{1,0:T(8,128)S(1)} %copy.28.cos_ref, ...), custom_call_target="tpu_custom_call" | custom-call | tf_op jit(solution)/shard_map/attend/pallas_call | solution.py:451
  74.4 0.0 copy-done
  74.4 0.0 copy-done.3
  74.5 0.0 copy-done.2
  74.5 33.1 %project.1 = bf16[4,96,256]{2,1,0:T(8,128)(2,1)S(1)} custom-call(bf16[4,384,256]{2,1,0:T(8,128)(2,1)S(1)} %get-tuple-element.5.part_ref, f32[384,128]{1,0:T(8,128)S(1)} %get-tuple-element.6.stats_ref, bf16[4,64,256]{2,1,0:T(8,128)(2,1)S(1)} %dynamic-slice_bitcast_fusion.wv_ref, bf16[256,256]{1,0:T(8,128)(2,1)S(1)} %copy-done.2, f32[1,256]{1,0:T(1,128)S(1)} %bitcast.20), custom_call_target="tpu_custom_call" | custom-call | tf_op jit(solution)/shard_map/project/pallas_call | solution.py:496
  107.6 0.7 copy.35
  (14 shorter events, 0.2 us)
Async XLA Ops:
  0.6 73.8 %copy-start = (bf16[16,256,64]{1,2,0:T(8,128)(2,1)S(1)}, bf16[16,256,64]{1,2,0:T(8,128)(2,1)}, u32[]{:S(2)}) copy-start(bf16[16,256,64]{1,2,0:T(8,128)(2,1)} %param.25) | copy-start | bytes 1572868
  0.6 73.8 %copy-start.3 = (bf16[256]{0:T(256)(128)(2,1)S(1)}, bf16[256]{0:T(256)(128)(2,1)}, u32[]{:S(2)}) copy-start(bf16[256]{0:T(256)(128)(2,1)} %param.27) | copy-start | bytes 1540
  0.7 73.8 %copy-start.2 = (bf16[256,256]{1,0:T(8,128)(2,1)S(1)}, bf16[256,256]{1,0:T(8,128)(2,1)}, u32[]{:S(2)}) copy-start(bf16[256,256]{1,0:T(8,128)(2,1)} %w_out_ref.1) | copy-start | bytes 393220
  47.1 1.3 %copy-start.1 = (bf16[512,4,288]{0,2,1:T(8,128)(2,1)S(1)}, bf16[512,4,288]{0,2,1:T(8,128)(2,1)}, u32[]{:S(2)}) copy-start(bf16[512,4,288]{0,2,1:T(8,128)(2,1)} %param.24) | copy-start | bytes 3538948
where the time goes:
time: 109 us; the launch traced here: 108 us
  Pallas kernels  96.4 us (88%)
  local copies, waits for them, and re-layouts  5.31 us (5%)
  other arithmetic  4.7 us (4%)
    pallas_call x1, Pallas kernels, local(): pl.pallas_call(functools.partial(compress_kernel, n_kv, n_tp, width, q_ra...  37.2 us
    pallas_call x1, Pallas kernels, local(): pl.pallas_call(functools.partial(project_kernel, n_kv, n_tp), name='proje...  33.1 us
    pallas_call x1, Pallas kernels, local(): pl.pallas_call(functools.partial(attend_kernel, group), name='attend', ou...  26.1 us
    unnamed x10, local copies, waits for them, and re-layouts  2.73 us

commit v1 on v0

v1 whole, which is shorter than its diff:
```python
import functools

import jax
import jax.numpy as jnp
from jax import lax
from jax.experimental import pallas as pl
from jax.experimental.pallas import tpu as pltpu
from jax.sharding import PartitionSpec as P

NOPE_DIM = 64
LANES = 128

epsilon = 1e-06
rope_base = 10000.0
score_after_mask = -1e30
MESH = pl.DeviceIdType.MESH
HIGHEST = lax.Precision.HIGHEST
VMEM = pl.BlockSpec(memory_space=pltpu.VMEM)


def dot(a, b, precision=None):
    return jnp.dot(a, b, preferred_element_type=jnp.float32, precision=precision)


def dot_nt(a, b, precision=None):
    return lax.dot_general(
        a, b, (((1,), (1,)), ((), ())), preferred_element_type=jnp.float32, precision=precision
    )


def remote(src, dst, send_sem, recv_sem, device_id):
    return pltpu.make_async_remote_copy(
        src_ref=src,
        dst_ref=dst,
        send_sem=send_sem,
        recv_sem=recv_sem,
        device_id=device_id,
        device_id_type=MESH,
    )


def root_mean(values, count):
    return lax.rsqrt(jnp.sum(values * values, axis=-1, keepdims=True) / count + epsilon)


def flip(index, bits):
    out = index
    bit = 1
    while bit <= bits:
        if bits & bit:
            out = out + bit - 2 * bit * lax.rem(lax.div(index, bit), 2)
        bit *= 2
    return out


def iota(shape, axis):
    return lax.broadcasted_iota(jnp.int32, shape, axis)


def row_table(lengths, accepted, parents, freq, rows):
    props, seqs = parents.shape
    spread = (lax.div(iota((seqs, rows), 1), props) == iota((seqs, rows), 0)).astype(jnp.float32)
    owner = lax.div(iota((1, rows), 1), props)
    filled = jnp.zeros((1, rows), jnp.int32)
    for s in range(seqs):
        filled = jnp.where(owner == s, lengths[s] + accepted[s], filled)
    filled = filled.astype(jnp.float32)
    links = dot(parents.astype(jnp.float32), spread, HIGHEST)
    own = lax.rem(iota((props, rows), 1), props) == iota((props, rows), 0)
    link = jnp.sum(jnp.where(own, links, 0.0), axis=0, keepdims=True)
    link = link.astype(jnp.int32)
    base = lax.div(iota((1, rows), 1), props) * props
    above = jnp.where(link < 0, -1, base + link)
    up_index = iota((rows, rows), 0)
    reached = jnp.where((up_index == above) | (up_index == iota((rows, rows), 1)), 1.0, 0.0)
    for repeat in range((props - 1).bit_length()):
        half = reached.astype(jnp.bfloat16)
        reached = jnp.minimum(dot(half, half), 1.0)
    compact = jnp.sum(reached.reshape(seqs, props, rows), axis=0)
    place = filled + jnp.sum(compact, axis=0, keepdims=True) - 1.0
    angles = place * freq
    cosine, sine = jnp.cos(angles), jnp.sin(angles)
    rest = LANES - 4 * freq.shape[0] - props
    table = jnp.concatenate(
        [cosine, cosine, -sine, sine, compact, jnp.zeros((rest, rows), jnp.float32)], axis=0
    )
    return table.T


def compress_kernel(
    n_kv, n_tp, few,
    x_hbm, wq_hbm, wk_hbm, gain_x_hbm, gain_q_hbm, gain_k_hbm, parents_hbm,
    lengths_hbm, accepted_hbm, freq_ref, expand_hbm, cache_hbm,
    q_all, k_all, table_ref, expand_ref, held_ref,
    x_own, wq_own, wk_raw, gain_x, gain_q, gain_k, parents_ref, lengths, accepted, wk_own, x_msg, got_x, got_wq, got_wk, part, got_part, sq_all,
    fetch_s, fetch_c,
    send_x, recv_x, send_w, recv_w, send_s, recv_s, send_p, recv_p,
    send_a, send_y, send_b, recv_q, recv_k,
):
    me_k, me_t = lax.axis_index("kv"), lax.axis_index("tp")
    n_y = n_tp // 2
    me_y, core = lax.div(me_t, 2), lax.rem(me_t, 2)
    mine = me_t * n_kv + me_k
    barrier = pltpu.get_barrier_semaphore()
    everyone = [(dk, dt) for dk in range(n_kv) for dt in range(n_tp) if dk or dt]
    for dk, dt in everyone:
        pl.semaphore_signal(
            barrier, inc=1,
            device_id={"kv": flip(me_k, dk), "tp": flip(me_t, dt)}, device_id_type=MESH,
        )
    small = [
        pltpu.make_async_copy(src, dst, fetch_s.at[n])
        for n, (src, dst) in enumerate(
            (
                (x_hbm, x_own), (gain_x_hbm, gain_x), (lengths_hbm, lengths),
                (accepted_hbm, accepted), (parents_hbm, parents_ref), (wk_hbm, wk_raw),
                (wq_hbm, wq_own), (gain_q_hbm, gain_q), (gain_k_hbm, gain_k),
            )
        )
    ]
    for copy in small:
        copy.start()
    big = [pltpu.make_async_copy(expand_hbm, expand_ref, fetch_s.at[9])] + [
        pltpu.make_async_copy(cache_hbm.at[s], held_ref.at[s], fetch_c.at[s])
        for s in range(cache_hbm.shape[0])
    ]
    for copy in small:
        copy.wait()

    features, rows = x_own.shape
    q_rank, kv_rank = gain_q.shape[-1], gain_k.shape[-1]
    whole, wide = wk_raw.shape[1], wk_own.shape[1]
    each, half = part.shape[1], x_msg.shape[1]
    raw = x_own[...].astype(jnp.float32)
    squares = jnp.sum(raw * raw, axis=0, keepdims=True)
    sq_all[mine] = jnp.zeros_like(sq_all[0])
    for n in range(rows // LANES):
        sq_all[mine, n : n + 1, :] = squares[:, n * LANES : (n + 1) * LANES]
    scaled = raw.T * gain_x[...].astype(jnp.float32)[None]
    for y in range(n_y):
        for n in range(2):
            blocks = []
            for j in range(n_kv // 2):
                start = (y * n_kv + n * (n_kv // 2) + j) * few
                blocks.append(scaled[start : start + few])
                if each > few:
                    blocks.append(jnp.zeros((each - few, features), jnp.float32))
            if each == few:
                start = (y * n_kv + n * (n_kv // 2)) * few
                blocks = [scaled[start : start + half]]
            value = jnp.concatenate(blocks, axis=0).astype(jnp.bfloat16)
            x_msg[y, :, n * features : (n + 1) * features] = value
    wk_own[...] = jnp.zeros_like(wk_own)
    wk_own[:, :whole] = wk_raw[...]
    pl.semaphore_wait(barrier, n_kv * n_tp - 1)

    def role(c):
        sends = []

        def start(*args):
            copy = remote(*args)
            copy.start()
            sends.append(copy)

        w_own, got_w, width = (wq_own, got_wq, q_rank) if c == 0 else (wk_own, got_wk, wide)
        for dt in reversed(range(1, n_tp)):
            peer = flip(me_t, dt)
            theirs, land = (wq_own, got_wq) if (c ^ dt) % 2 == 0 else (wk_own, got_wk)
            start(theirs, land.at[me_t], send_w.at[dt], recv_w.at[me_t], {"tp": peer})
            start(
                x_msg.at[lax.div(peer, 2)], got_x.at[me_t], send_x.at[dt], recv_x.at[me_t],
                {"tp": peer},
            )
        for n, (dk, dt) in enumerate(everyone):
            start(
                sq_all.at[mine], sq_all.at[mine], send_s.at[n], recv_s.at[mine],
                {"kv": flip(me_k, dk), "tp": flip(me_t, dt)},
            )
        for copy in big:
            copy.start()
        table_ref[:rows] = row_table(
            lengths, accepted, parents_ref[...], freq_ref[...], rows
        )

        for dt in range(1, n_tp):
            peer = flip(me_t, dt)
            remote(w_own, got_w.at[peer], send_w.at[dt], recv_w.at[peer], {"tp": peer}).wait_recv()
            remote(
                x_msg.at[0], got_x.at[peer], send_x.at[dt], recv_x.at[peer], {"tp": peer}
            ).wait_recv()
        terms = [(x_msg[me_y], w_own[...])]
        for dt in range(1, n_tp):
            peer = flip(me_t, dt)
            terms.append((got_x[peer], got_w[peer]))
        for n in range(2):
            total = None
            for x, w in terms:
                term = dot(x[:, n * features : (n + 1) * features], w)
                total = term if total is None else total + term
            for j in range(n_kv // 2):
                part[n * (n_kv // 2) + j, :, :width] = total[j * each : (j + 1) * each]

        cut = pl.ds(0, width)
        for dk in reversed(range(1, n_kv)):
            peer = flip(me_k, dk)
            start(
                part.at[peer, :, cut], got_part.at[me_k, :, cut], send_p.at[dk],
                recv_p.at[me_k], {"kv": peer},
            )
        block = me_y * n_kv + me_k
        first = block * few
        for n, (dk, dt) in enumerate(everyone):
            source = flip(me_t, dt) * n_kv + flip(me_k, dk)
            remote(
                sq_all.at[source], sq_all.at[source], send_s.at[n], recv_s.at[source],
                {"kv": flip(me_k, dk), "tp": flip(me_t, dt)},
            ).wait_recv()
        square = sq_all[0]
        for n in range(1, n_kv * n_tp):
            square = square + sq_all[n]
        column = jnp.zeros((each, 1), jnp.float32)
        for n in range(rows // LANES):
            here = iota((each, LANES), 1) + n * LANES == iota((each, LANES), 0) + first
            column = column + jnp.sum(
                jnp.where(here, square[n : n + 1], 0.0), axis=1, keepdims=True
            )
        inverse = lax.rsqrt(column / (n_kv * n_tp * features) + epsilon)
        summed = part[me_k, :, :width]
        for dk in range(1, n_kv):
            peer = flip(me_k, dk)
            remote(
                part.at[peer, :, cut], got_part.at[peer, :, cut], send_p.at[dk],
                recv_p.at[peer], {"kv": peer},
            ).wait_recv()
            summed = summed + got_part[peer, :, :width]
        if c == 0:
            query = summed * inverse
            query = query * root_mean(query, q_rank) * gain_q[...].astype(jnp.float32)[None]
            q_all[block] = query.astype(jnp.bfloat16)
        else:
            latent = summed[:, :kv_rank] * inverse
            latent = latent * root_mean(latent, kv_rank) * gain_k[...].astype(jnp.float32)[None]
            k_all[block, :, :kv_rank] = latent.astype(jnp.bfloat16)
            turn = summed[:, kv_rank:] * inverse
            turn_dim = whole - kv_rank
            lane = iota(turn.shape, 1)
            swapped = jnp.where(
                lane < turn_dim // 2,
                pltpu.roll(turn, LANES - turn_dim // 2, 1),
                pltpu.roll(turn, turn_dim // 2, 1),
            )
            angles = table_ref[pl.ds(first, each), :]
            turned = turn * angles + swapped * pltpu.roll(angles, LANES - turn_dim, 1)
            turned = jnp.where(lane < turn_dim, turned, 0.0)
            k_all[block, :, kv_rank:] = turned.astype(jnp.bfloat16)

        ours, recv_ours = (q_all, recv_q) if c == 0 else (k_all, recv_k)
        other, recv_other = (k_all, recv_k) if c == 0 else (q_all, recv_q)
        sibling = me_t + 1 - 2 * c

        def send(n, sem, device_id):
            start(ours.at[n], ours.at[n], sem, recv_ours.at[n], device_id)

        def landed(buf, n, recv):
            remote(buf.at[n], buf.at[n], send_a.at[0], recv.at[n], {"tp": sibling}).wait_recv()

        for dk in reversed(range(1, n_kv)):
            send(block, send_a.at[dk], {"kv": flip(me_k, dk)})
        for dk in range(n_kv):
            here = me_y * n_kv + flip(me_k, dk)
            if dk:
                landed(ours, here, recv_ours)
            for dy in range(1, n_y):
                send(here, send_y.at[dy * n_kv + dk], {"tp": flip(me_t, 2 * dy)})
            send(here, send_b.at[dk], {"tp": sibling})
        for dy in range(1, n_y):
            for dk in range(n_kv):
                here = flip(me_y, dy) * n_kv + flip(me_k, dk)
                landed(ours, here, recv_ours)
                send(here, send_b.at[dy * n_kv + dk], {"tp": sibling})
        for dy in range(n_y):
            for dk in range(n_kv):
                landed(other, flip(me_y, dy) * n_kv + flip(me_k, dk), recv_other)
        for copy in big:
            copy.wait()
        for copy in sends:
            copy.wait_send()

    for c in range(2):
        pl.when(core == c)(functools.partial(role, c))


def attend_kernel(
    group, lengths_ref, accepted_ref, low_ref, fresh_ref, table_ref, wq_ref, held_in,
    out_hbm, part_ref, stats_ref, held_ref, q_main, q_turn, bias, write,
):
    heads, whole, _ = wq_ref.shape
    seqs, _, span = held_ref.shape
    rank = part_ref.shape[-1]
    turn_dim = whole - rank
    half = turn_dim // 2
    props = q_main.shape[1] // heads
    scale = (NOPE_DIM + turn_dim) ** (-0.5)
    rows = low_ref.shape[0]
    offset = lax.axis_index("kv") * span

    low = low_ref[...]
    cosine = table_ref[:rows, :turn_dim]
    sine = table_ref[:rows, turn_dim : 2 * turn_dim]
    for h in range(heads):
        main = dot_nt(low, wq_ref[h, :rank, :])
        front, back = wq_ref[h, rank : rank + half, :], wq_ref[h, rank + half :, :]
        turn = dot_nt(low, jnp.concatenate([front, back], axis=0))
        swapped = dot_nt(low, jnp.concatenate([back, front], axis=0))
        turned = turn * cosine + swapped * sine
        lines = slice(h * props, (h + 1) * props)
        q_main[:, lines, :] = main.astype(jnp.bfloat16).reshape(seqs, props, rank)
        q_turn[:, lines, :] = turned.astype(jnp.bfloat16).reshape(seqs, props, turn_dim)

    def patch(s, carry):
        rel = lengths_ref[s] + accepted_ref[s] - offset
        lines = pl.ds(pl.multiple_of(s * props, props), props)
        first = lax.shift_right_arithmetic(rel, 7)
        last = lax.shift_right_arithmetic(rel + props - 1, 7)
        for more in range(2):
            chunk = first + more

            @pl.when((chunk >= 0) & (chunk < span // LANES) & (chunk <= last))
            def _():
                start = pl.multiple_of(chunk * LANES, LANES)
                slot = start - rel + iota((props, LANES), 1)
                onehot = (slot == iota((props, LANES), 0)).astype(jnp.float32).astype(jnp.bfloat16)
                placed = lax.dot_general(
                    fresh_ref[lines, :whole], onehot, (((0,), (0,)), ((), ())),
                    preferred_element_type=jnp.float32,
                )
                slots = start - rel + iota(placed.shape, 1)
                old = held_ref[s, :, pl.ds(start, LANES)].astype(jnp.float32)
                new = jnp.where((slots >= 0) & (slots < props), placed, old)
                held_ref[s, :, pl.ds(start, LANES)] = new.astype(jnp.bfloat16)

        return carry

    lax.fori_loop(0, seqs, patch, 0)

    def write_out(s):
        return pltpu.make_async_copy(held_ref.at[s], out_hbm.at[s], write.at[s])

    for s in range(seqs):
        write_out(s).start()

    def step(i, carry):
        for g in range(group):
            s = i * group + g
            rel = lengths_ref[s] + accepted_ref[s] - offset
            lines = pl.ds(pl.multiple_of(s * props, props), props)
            past = iota((props, span), 1) < rel
            bias[g] = jnp.where(past, 0.0, score_after_mask)
            first = lax.shift_right_arithmetic(rel, 7)
            last = lax.shift_right_arithmetic(rel + props - 1, 7)
            for more in range(2):
                chunk = first + more

                @pl.when((chunk >= 0) & (chunk < span // LANES) & (chunk <= last))
                def _():
                    start = pl.multiple_of(chunk * LANES, LANES)
                    slot = start - rel + iota((props, LANES), 1)
                    onehot = slot == iota((props, LANES), 0)
                    onehot = onehot.astype(jnp.float32).astype(jnp.bfloat16)
                    reached = table_ref[lines, 2 * turn_dim : 2 * turn_dim + props]
                    seen = (slot < 0) | (dot(reached.astype(jnp.bfloat16), onehot) > 0.5)
                    bias[g, :, pl.ds(start, LANES)] = jnp.where(seen, 0.0, score_after_mask)

        for g in range(group):
            s = i * group + g
            scores = dot(q_main[s], held_ref[s, :rank, :]) + dot(q_turn[s], held_ref[s, rank:, :])
            masked = scores.reshape(heads, props, span) * scale + bias[g][None]
            top = jnp.max(masked, axis=-1, keepdims=True)
            weights = jnp.exp(masked - jnp.maximum(top, -1e29))
            totals = jnp.sum(weights, axis=-1, keepdims=True)
            prob = weights.astype(jnp.bfloat16).reshape(heads * props, span)
            weighted = dot_nt(prob, held_ref[s, :rank, :]).reshape(heads, props, rank)
            part = (weighted / jnp.maximum(totals, 1.0)).astype(jnp.bfloat16)
            lane = iota((props, LANES), 1)
            stats = jnp.zeros((props, LANES), jnp.float32)
            lines = pl.ds(pl.multiple_of(s * props, props), props)
            for h in range(heads):
                part_ref[h, lines, :] = part[h]
                stats = jnp.where(lane == h, top[h], stats)
                stats = jnp.where(lane == heads + h, totals[h], stats)
            stats_ref[lines, :] = stats
        return carry

    lax.fori_loop(0, seqs // group, step, 0)
    for s in range(seqs):
        write_out(s).wait()


def project_kernel(
    n_kv, n_tp,
    part_ref, stats_ref, wv_ref, w_out_ref, gain_ref, out_ref,
    vals, stat, got_vals, got_stat, attended, raw, got_raw, sums, result,
    send_v, recv_v, send_s, recv_s, send_a, recv_a, send_r, recv_r, send_q, recv_q, send_o, recv_o,
):
    me_k, me_t = lax.axis_index("kv"), lax.axis_index("tp")
    heads, _, _ = part_ref.shape
    v_dim = wv_ref.shape[1]
    kv_peers = [lax.rem(me_k + d, n_kv) for d in range(n_kv)]
    tp_peers = [lax.rem(me_t + d, n_tp) for d in range(n_tp)]
    barrier = pltpu.get_barrier_semaphore()
    for dk in range(n_kv):
        for dt in range(n_tp):
            if dk or dt:
                pl.semaphore_signal(
                    barrier, inc=1,
                    device_id={"kv": kv_peers[dk], "tp": tp_peers[dt]}, device_id_type=MESH,
                )
    sends = []

    each = vals.shape[1]
    line = lax.broadcasted_iota(jnp.int32, (16, LANES), 0)
    lane = lax.broadcasted_iota(jnp.int32, (16, LANES), 1)
    tops = (line < heads) & (lane == line)
    counts = (line >= 8) & (line < 8 + heads) & (lane == line - 8 + heads)
    pick = jnp.where(tops | counts, 1.0, 0.0)
    values = jnp.concatenate([dot_nt(part_ref[h], wv_ref[h]) for h in range(heads)], axis=1)
    for j in range(n_kv):
        vals[j] = values[j * each : (j + 1) * each].astype(jnp.bfloat16)
        stat[j] = dot_nt(pick, stats_ref[j * each : (j + 1) * each, :], HIGHEST)
    pl.semaphore_wait(barrier, n_kv * n_tp - 1)

    def exchange(axis, peers, src_of, dst, own, send_sem, recv_sem):
        for d in range(1, len(peers)):
            copy = remote(
                src_of(peers[d]), dst.at[own], send_sem.at[d], recv_sem.at[own], {axis: peers[d]}
            )
            copy.start()
            sends.append(copy)

    def arrived(axis, peers, d, src_of, dst, send_sem, recv_sem):
        remote(
            src_of(peers[d]), dst.at[peers[d]], send_sem.at[d], recv_sem.at[peers[d]],
            {axis: peers[d]},
        ).wait_recv()

    exchange("kv", kv_peers, lambda p: stat.at[p], got_stat, me_k, send_s, recv_s)
    exchange("kv", kv_peers, lambda p: vals.at[p], got_vals, me_k, send_v, recv_v)
    for d in range(1, n_kv):
        arrived("kv", kv_peers, d, lambda p: stat.at[p], got_stat, send_s, recv_s)
    all_stats = [stat[me_k]] + [got_stat[p] for p in kv_peers[1:]]
    largest = all_stats[0][:8]
    for one in all_stats[1:]:
        largest = jnp.maximum(largest, one[:8])
    shares = jnp.concatenate([one[8:] * jnp.exp(one[:8] - largest) for one in all_stats], axis=0)
    turn_eye = lax.broadcasted_iota(jnp.int32, (each, each), 0) == lax.broadcasted_iota(
        jnp.int32, (each, each), 1
    )
    shares = dot_nt(turn_eye.astype(jnp.float32), shares, HIGHEST)
    wide = lax.broadcasted_iota(jnp.int32, (each, heads * v_dim), 1)

    def spread(d):
        out = shares[:, 8 * d : 8 * d + 1]
        for h in range(1, heads):
            out = jnp.where(wide >= h * v_dim, shares[:, 8 * d + h : 8 * d + h + 1], out)
        return jnp.broadcast_to(out, wide.shape)

    summed = None
    for d in range(n_kv):
        share = spread(d)
        if d:
            arrived("kv", kv_peers, d, lambda p: vals.at[p], got_vals, send_v, recv_v)
        block = got_vals[kv_peers[d]] if d else vals[me_k]
        term = share * block.astype(jnp.float32)
        summed = term if summed is None else summed + term
        weight = share if d == 0 else weight + share
    attended[me_k] = (summed / weight).astype(jnp.bfloat16)
    exchange("kv", kv_peers, lambda p: attended.at[me_k], attended, me_k, send_a, recv_a)
    for d in range(1, n_kv):
        arrived("kv", kv_peers, d, lambda p: attended.at[p], attended, send_a, recv_a)

    lines = jnp.concatenate([attended[j].astype(jnp.float32) for j in range(n_kv)], axis=0)
    lines = dot(lines.astype(jnp.bfloat16), w_out_ref[...])
    share_rows, cols = raw.shape[1:]
    for t in range(n_tp):
        raw[t] = lines[t * share_rows : (t + 1) * share_rows].astype(jnp.bfloat16)
    exchange("tp", tp_peers, lambda p: raw.at[p], got_raw, me_t, send_r, recv_r)
    mixed = raw[me_t].astype(jnp.float32)
    for d in range(1, n_tp):
        arrived("tp", tp_peers, d, lambda p: raw.at[p], got_raw, send_r, recv_r)
        mixed = mixed + got_raw[tp_peers[d]].astype(jnp.float32)
    result[me_t] = mixed.astype(jnp.bfloat16)
    exchange("tp", tp_peers, lambda p: result.at[me_t], result, me_t, send_o, recv_o)
    mine = me_t * n_kv + me_k
    sums[mine] = dot_nt(jnp.ones((8, cols), jnp.float32), mixed * mixed, HIGHEST)
    everyone = [(dk, dt) for dt in range(n_tp) for dk in range(n_kv) if dk or dt]
    for n, (dk, dt) in enumerate(everyone):
        copy = remote(
            sums.at[mine], sums.at[mine], send_q.at[n], recv_q.at[mine],
            {"kv": kv_peers[dk], "tp": tp_peers[dt]},
        )
        copy.start()
        sends.append(copy)
    for n, (dk, dt) in enumerate(everyone):
        source = tp_peers[dt] * n_kv + kv_peers[dk]
        remote(
            sums.at[source], sums.at[source], send_q.at[n], recv_q.at[source],
            {"kv": kv_peers[dk], "tp": tp_peers[dt]},
        ).wait_recv()
    eye = iota((share_rows, share_rows), 0) == iota((share_rows, share_rows), 1)
    for d in range(1, n_tp):
        arrived("tp", tp_peers, d, lambda p: result.at[p], result, send_o, recv_o)
    for t in range(n_tp):
        square = sums[t * n_kv]
        for j in range(1, n_kv):
            square = square + sums[t * n_kv + j]
        norm = lax.rsqrt(square / (cols * n_kv) + epsilon)
        column = jnp.sum(jnp.where(eye, norm[:1], 0.0), axis=1, keepdims=True)
        out_ref[t] = (result[t].astype(jnp.float32) * column * gain_ref[...]).astype(jnp.bfloat16)
    for copy in sends:
        copy.wait_send()


def up(value, to):
    return -(-value // to) * to


def local(
    n_kv,
    n_tp,
    activations,
    latent_cache,
    lengths,
    accepted,
    parents,
    w_query_down,
    w_key_down,
    gain_input,
    gain_query,
    gain_key,
    w_query,
    w_value,
    w_out,
    gain_output,
):
    bf16, f32 = jnp.bfloat16, jnp.float32
    seqs, props = parents.shape
    rows, features = activations.shape
    heads = w_query.shape[1]
    q_rank, kv_rank = gain_query.shape[0], gain_key.shape[0]
    whole = latent_cache.shape[-1]
    turn_dim = whole - kv_rank
    half = turn_dim // 2
    span = latent_cache.shape[1]
    v_dim = w_value.shape[-1]
    cols = w_out.shape[1]
    n_dev = n_kv * n_tp
    me_t = lax.axis_index("tp")

    n_y = n_tp // 2
    blocks = n_y * n_kv
    few = rows // blocks
    each = up(few, 8)
    wide = up(whole, LANES)
    frequency = rope_base ** (-jnp.arange(half, dtype=f32) / half)
    dma = pltpu.SemaphoreType.DMA
    hbm = pl.BlockSpec(memory_space=pl.ANY)
    far = lambda array: pltpu.with_memory_space_constraint(array, pltpu.HBM)
    q_all, k_all, table, expand, held = pl.pallas_call(
        functools.partial(compress_kernel, n_kv, n_tp, few),
        name="compress",
        out_shape=(
            jax.ShapeDtypeStruct((blocks, each, q_rank), bf16),
            jax.ShapeDtypeStruct((blocks, each, wide), bf16),
            jax.ShapeDtypeStruct((rows + 8, LANES), f32),
            pltpu.VMEM((heads, whole, q_rank), bf16),
            pltpu.VMEM((seqs, whole, span), bf16),
        ),
        in_specs=[hbm] * 9 + [VMEM] + [hbm] * 2,
        out_specs=(VMEM,) * 5,
        scratch_shapes=[
            pltpu.VMEM((features, rows), bf16),
            pltpu.VMEM((features, q_rank), bf16),
            pltpu.VMEM((features, whole), bf16),
            pltpu.VMEM((features,), bf16),
            pltpu.VMEM((q_rank,), bf16),
            pltpu.VMEM((kv_rank,), bf16),
            pltpu.VMEM((props, seqs), jnp.int32),
            pltpu.SMEM((seqs,), jnp.int32),
            pltpu.SMEM((seqs,), jnp.int32),
            pltpu.VMEM((features, wide), bf16),
            pltpu.VMEM((n_y, n_kv * each // 2, 2 * features), bf16),
            pltpu.VMEM((n_tp, n_kv * each // 2, 2 * features), bf16),
            pltpu.VMEM((n_tp, features, q_rank), bf16),
            pltpu.VMEM((n_tp, features, wide), bf16),
            pltpu.VMEM((n_kv, each, max(q_rank, wide)), f32),
            pltpu.VMEM((n_kv, each, max(q_rank, wide)), f32),
            pltpu.VMEM((n_dev, 8, LANES), f32),
            dma((10,)), dma((seqs,)),
            dma((n_tp,)), dma((n_tp,)), dma((n_tp,)), dma((n_tp,)),
            dma((n_dev,)), dma((n_dev,)), dma((n_kv,)), dma((n_kv,)),
            dma((n_kv,)), dma((blocks,)), dma((blocks,)), dma((blocks,)), dma((blocks,)),
        ],
        compiler_params=pltpu.CompilerParams(
            collective_id=0, has_side_effects=True, vmem_limit_bytes=20 * 1024 * 1024
        ),
    )(
        far(activations.T), far(w_query_down), far(w_key_down),
        far(gain_input), far(gain_query), far(gain_key), far(parents.T),
        far(lengths), far(accepted), frequency[:, None],
        far(w_query.transpose(1, 2, 0)), far(latent_cache.transpose(0, 2, 1)),
    )
    query_low = q_all[:, :few].reshape(rows, q_rank)
    fresh = k_all[:, :few].reshape(rows, wide)

    group = next(g for g in (3, 2, 1) if seqs % g == 0)
    smem = pl.BlockSpec(memory_space=pltpu.SMEM)
    updated, part, stats, _ = pl.pallas_call(
        functools.partial(attend_kernel, group),
        name="attend",
        out_shape=(
            jax.ShapeDtypeStruct((seqs, whole, span), bf16),
            jax.ShapeDtypeStruct((heads, rows, kv_rank), bf16),
            jax.ShapeDtypeStruct((rows, LANES), f32),
            pltpu.VMEM((seqs, whole, span), bf16),
        ),
        in_specs=[smem] * 2 + [VMEM] * 5,
        out_specs=(hbm, VMEM, VMEM, VMEM),
        scratch_shapes=[
            pltpu.VMEM((seqs, heads * props, kv_rank), bf16),
            pltpu.VMEM((seqs, heads * props, turn_dim), bf16),
            pltpu.VMEM((group, props, span), f32),
            dma((seqs,)),
        ],
        input_output_aliases={6: 3},
        compiler_params=pltpu.CompilerParams(vmem_limit_bytes=24 * 1024 * 1024),
    )(
        lengths, accepted, query_low, fresh, table,
        pltpu.with_memory_space_constraint(expand, pltpu.VMEM),
        pltpu.with_memory_space_constraint(held, pltpu.VMEM),
    )

    wv = lax.dynamic_slice_in_dim(w_value.transpose(0, 2, 1), me_t * heads, heads, 0)
    per_kv, per_tp = rows // n_kv, rows // n_tp
    mixed = pl.pallas_call(
        functools.partial(project_kernel, n_kv, n_tp),
        name="project",
        out_shape=jax.ShapeDtypeStruct((n_tp, per_tp, cols), bf16),
        in_specs=[VMEM] * 5,
        out_specs=VMEM,
        scratch_shapes=[
            pltpu.VMEM((n_kv, per_kv, heads * v_dim), bf16),
            pltpu.VMEM((n_kv, 16, per_kv), f32),
            pltpu.VMEM((n_kv, per_kv, heads * v_dim), bf16),
            pltpu.VMEM((n_kv, 16, per_kv), f32),
            pltpu.VMEM((n_kv, per_kv, heads * v_dim), bf16),
            pltpu.VMEM((n_tp, per_tp, cols), bf16),
            pltpu.VMEM((n_tp, per_tp, cols), bf16),
            pltpu.VMEM((n_dev, 8, per_tp), f32),
            pltpu.VMEM((n_tp, per_tp, cols), bf16),
            dma((n_kv,)), dma((n_kv,)), dma((n_kv,)), dma((n_kv,)), dma((n_kv,)), dma((n_kv,)),
            dma((n_tp,)), dma((n_tp,)), dma((n_dev,)), dma((n_dev,)), dma((n_tp,)), dma((n_tp,)),
        ],
        compiler_params=pltpu.CompilerParams(
            collective_id=1, has_side_effects=True, vmem_limit_bytes=32 * 1024 * 1024
        ),
    )(part, stats, wv, w_out, gain_output.astype(f32)[None])
    return (mixed.reshape(rows, cols), updated.transpose(0, 2, 1))


def solution(mesh):
    in_specs = (
        P(None, ("kv", "tp")),
        P(None, "kv", None),
        P(),
        P(),
        P(),
        P(("kv", "tp"), None),
        P(("kv", "tp"), None),
        P(("kv", "tp")),
        P(),
        P(),
        P(None, "tp", None),
        P(),
        P("tp", "kv"),
        P("kv"),
    )
    out_specs = (P(None, "kv"), P(None, "kv", None))
    body = functools.partial(local, mesh.shape["kv"], mesh.shape["tp"])
    return jax.shard_map(body, mesh=mesh, in_specs=in_specs, out_specs=out_specs, check_vma=False)
```

time: 109 us -> 87 us (0.80)
  Pallas kernels: 96.4 us -> 84.4 us
  other arithmetic: 4.7 us -> 0.02 us
  local copies, waits for them, and re-layouts: 5.31 us -> 0.73 us
    pallas_call x1, Pallas kernels: 26.1 us -> 21.1 us  [local(): pl.pallas_call(functools.partial(attend_kernel, group), name='attend', ou...]
    pallas_call x1, Pallas kernels: 37.2 us -> 33.7 us  [local(): pl.pallas_call(functools.partial(compress_kernel, n_kv, n_tp, few), name=...]
    pallas_call x1, Pallas kernels: 33.1 us -> 29.7 us  [local(): pl.pallas_call(functools.partial(project_kernel, n_kv, n_tp), name='proje...]
    unnamed x10 -> x11, local copies, waits for them, and re-layouts: 2.73 us -> 0.71 us
    convert_element_type x4 -> x0, other arithmetic: 1.61 us -> none  [the longest x2 1.53 us: local(): scaled = (activations.astype(f32) * gain_input.astype(f32)).astype(bf16)]
    broadcast_in_dim x2 -> x0, other arithmetic: 1.34 us -> none  [the longest x1 0.68 us: local(): gain_query.astype(f32)[None]]
    concatenate x4 -> x0, local copies, waits for them, and re-layouts: 1.31 us -> none  [the longest x1 0.94 us: local(): jnp.concatenate([w_query_down, w_key_down, w_key_down[:, kv_rank + half:]...]
where the time goes in v1:
time: 87 us; the launch traced here: 85.9 us
  Pallas kernels  84.4 us (97%)
    pallas_call x1, Pallas kernels, local(): pl.pallas_call(functools.partial(compress_kernel, n_kv, n_tp, few), name=...  33.7 us
    pallas_call x1, Pallas kernels, local(): pl.pallas_call(functools.partial(project_kernel, n_kv, n_tp), name='proje...  29.7 us
    pallas_call x1, Pallas kernels, local(): pl.pallas_call(functools.partial(attend_kernel, group), name='attend', ou...  21.1 us

profile of v1, /device:TPU:0, one launch (start us, length us, event | category | flops | bytes accessed | tf_op | source)
XLA Modules:
  0.0 85.9 jit_solution(137189124228457989)
XLA Ops:
  0.6 0.0 copy-start
  0.6 0.0 copy-start.2
  0.7 0.0 copy-start.3
  0.7 0.0 copy-start.4
  0.7 0.0 copy-start.1
  0.7 33.7 %compress.1 = (bf16[16,24,512]{2,1,0:T(8,128)(2,1)S(1)}, bf16[16,24,384]{2,1,0:T(8,128)(2,1)S(1)}, f32[392,128]{1,0:T(8,128)S(1)}, bf16[4,288,512]{2,1,0:T(8,128)(2,1)S(1)}, bf16[24,288,2048]{2,1,0:T(8,128)(2,1)S(1)}) custom-call(bf16[64,384]{1,0:T(8,128)(2,1)} %bitcast.17, bf16[64,512]{1,0:T(8,128)(2,1)} %wq_hbm.1, bf16[64,288]{1,0:T(8,128)(2,1)} %wk_hbm.1, ...), custom_call_target="tpu_custom_call" | custom-call | tf_op jit(solution)/shard_map/compress/pallas_call | solution.py:568
  34.4 0.0 copy-done.2
  34.4 0.0 copy-done.3
  34.4 21.1 %attend.1 = (bf16[24,288,2048]{2,1,0:T(8,128)(2,1)}, bf16[4,384,256]{2,1,0:T(8,128)(2,1)S(1)}, f32[384,128]{1,0:T(8,128)S(1)}, bf16[24,288,2048]{2,1,0:T(8,128)(2,1)S(1)}) custom-call(s32[24]{0:T(128)S(1)} %copy-done.2, s32[24]{0:T(128)S(1)} %copy-done.3, bf16[384,512]{1,0:T(8,128)(2,1)S(1)} %bitcast.12, ...), custom_call_target="tpu_custom_call", output_to_operand_aliasing={{3}: (6, {})} | custom-call | tf_op jit(solution)/shard_map/attend/pallas_call | solution.py:617
  55.5 0.0 copy-done
  55.6 0.0 copy-done.4
  55.6 0.0 copy-done.1
  55.6 29.7 %project.1 = bf16[4,96,256]{2,1,0:T(8,128)(2,1)S(1)} custom-call(bf16[4,384,256]{2,1,0:T(8,128)(2,1)S(1)} %get-tuple-element.15.part_ref, f32[384,128]{1,0:T(8,128)S(1)} %get-tuple-element.16.stats_ref, bf16[4,64,256]{2,1,0:T(8,128)(2,1)S(1)} %dynamic-slice_bitcast_fusion.wv_ref, bf16[256,256]{1,0:T(8,128)(2,1)S(1)} %copy-done.1, f32[1,256]{1,0:T(1,128)S(1)} %bitcast.14), custom_call_target="tpu_custom_call" | custom-call | tf_op jit(solution)/shard_map/project/pallas_call | solution.py:644
  85.3 0.7 copy.19
  (3 shorter events, 0.0 us)
Async XLA Ops:
  0.6 54.9 %copy-start = (bf16[16,256,64]{1,2,0:T(8,128)(2,1)S(1)}, bf16[16,256,64]{1,2,0:T(8,128)(2,1)}, u32[]{:S(2)}) copy-start(bf16[16,256,64]{1,2,0:T(8,128)(2,1)} %param.25) | copy-start | bytes 1572868
  0.6 33.7 %copy-start.2 = (s32[24]{0:T(128)S(1)}, s32[24]{0:T(128)}, u32[]{:S(2)}) copy-start(s32[24]{0:T(128)} %lengths_ref.1) | copy-start | bytes 292
  0.7 33.7 %copy-start.3 = (s32[24]{0:T(128)S(1)}, s32[24]{0:T(128)}, u32[]{:S(2)}) copy-start(s32[24]{0:T(128)} %accepted_ref.1) | copy-start | bytes 292
  0.7 54.9 %copy-start.4 = (bf16[256]{0:T(256)(128)(2,1)S(1)}, bf16[256]{0:T(256)(128)(2,1)}, u32[]{:S(2)}) copy-start(bf16[256]{0:T(256)(128)(2,1)} %param.27) | copy-start | bytes 1540
  0.7 54.9 %copy-start.1 = (bf16[256,256]{1,0:T(8,128)(2,1)S(1)}, bf16[256,256]{1,0:T(8,128)(2,1)}, u32[]{:S(2)}) copy-start(bf16[256,256]{1,0:T(8,128)(2,1)} %w_out_ref.1) | copy-start | bytes 393220

commit v2 on v1

--- a/solution.py
+++ b/solution.py
@@ -292,7 +292,7 @@
 
 def attend_kernel(
     group, lengths_ref, accepted_ref, low_ref, fresh_ref, table_ref, wq_ref, held_in,
-    out_hbm, part_ref, stats_ref, held_ref, q_main, q_turn, bias, write,
+    out_hbm, part_ref, stats_ref, held_ref, q_main, q_turn, bias, turned_ref, write,
 ):
     heads, whole, _ = wq_ref.shape
     seqs, _, span = held_ref.shape
@@ -300,7 +300,7 @@
     turn_dim = whole - rank
     half = turn_dim // 2
     props = q_main.shape[1] // heads
-    scale = (NOPE_DIM + turn_dim) ** (-0.5)
+    power = (NOPE_DIM + turn_dim) ** (-0.5) * 1.4426950408889634
     rows = low_ref.shape[0]
     offset = lax.axis_index("kv") * span
 
@@ -320,6 +320,8 @@
     def patch(s, carry):
         rel = lengths_ref[s] + accepted_ref[s] - offset
         lines = pl.ds(pl.multiple_of(s * props, props), props)
+        past = iota((props, span), 1) < rel
+        bias[s] = jnp.where(past, 0.0, score_after_mask * 1.5)
         first = lax.shift_right_arithmetic(rel, 7)
         last = lax.shift_right_arithmetic(rel + props - 1, 7)
         for more in range(2):
@@ -330,6 +332,9 @@
                 start = pl.multiple_of(chunk * LANES, LANES)
                 slot = start - rel + iota((props, LANES), 1)
                 onehot = (slot == iota((props, LANES), 0)).astype(jnp.float32).astype(jnp.bfloat16)
+                reached = table_ref[lines, 2 * turn_dim : 2 * turn_dim + props]
+                seen = (slot < 0) | (dot(reached.astype(jnp.bfloat16), onehot) > 0.5)
+                bias[s, :, pl.ds(start, LANES)] = jnp.where(seen, 0.0, score_after_mask * 1.5)
                 placed = lax.dot_general(
                     fresh_ref[lines, :whole], onehot, (((0,), (0,)), ((), ())),
                     preferred_element_type=jnp.float32,
@@ -350,36 +355,18 @@
         write_out(s).start()
 
     def step(i, carry):
-        for g in range(group):
-            s = i * group + g
-            rel = lengths_ref[s] + accepted_ref[s] - offset
-            lines = pl.ds(pl.multiple_of(s * props, props), props)
-            past = iota((props, span), 1) < rel
-            bias[g] = jnp.where(past, 0.0, score_after_mask)
-            first = lax.shift_right_arithmetic(rel, 7)
-            last = lax.shift_right_arithmetic(rel + props - 1, 7)
-            for more in range(2):
-                chunk = first + more
-
-                @pl.when((chunk >= 0) & (chunk < span // LANES) & (chunk <= last))
-                def _():
-                    start = pl.multiple_of(chunk * LANES, LANES)
-                    slot = start - rel + iota((props, LANES), 1)
-                    onehot = slot == iota((props, LANES), 0)
-                    onehot = onehot.astype(jnp.float32).astype(jnp.bfloat16)
-                    reached = table_ref[lines, 2 * turn_dim : 2 * turn_dim + props]
-                    seen = (slot < 0) | (dot(reached.astype(jnp.bfloat16), onehot) > 0.5)
-                    bias[g, :, pl.ds(start, LANES)] = jnp.where(seen, 0.0, score_after_mask)
-
-        for g in range(group):
-            s = i * group + g
+        def score_of(s):
             scores = dot(q_main[s], held_ref[s, :rank, :]) + dot(q_turn[s], held_ref[s, rank:, :])
-            masked = scores.reshape(heads, props, span) * scale + bias[g][None]
+            return scores.reshape(heads, props, span) * power + bias[s][None]
+
+        def finish(s, g, masked):
             top = jnp.max(masked, axis=-1, keepdims=True)
-            weights = jnp.exp(masked - jnp.maximum(top, -1e29))
+            weights = jnp.exp2(masked - jnp.maximum(top, -1e29))
             totals = jnp.sum(weights, axis=-1, keepdims=True)
             prob = weights.astype(jnp.bfloat16).reshape(heads * props, span)
-            weighted = dot_nt(prob, held_ref[s, :rank, :]).reshape(heads, props, rank)
+            turned_ref[g] = held_ref[s, :rank, :].T
+            weighted = dot(prob, turned_ref[g]).reshape(heads, props, rank)
+            top = jnp.maximum(top * 0.6931471805599453, score_after_mask)
             part = (weighted / jnp.maximum(totals, 1.0)).astype(jnp.bfloat16)
             lane = iota((props, LANES), 1)
             stats = jnp.zeros((props, LANES), jnp.float32)
@@ -389,6 +376,10 @@
                 stats = jnp.where(lane == h, top[h], stats)
                 stats = jnp.where(lane == heads + h, totals[h], stats)
             stats_ref[lines, :] = stats
+
+        maskeds = [score_of(i * group + g) for g in range(group)]
+        for g in range(group):
+            finish(i * group + g, g, maskeds[g])
         return carry
 
     lax.fori_loop(0, seqs // group, step, 0)
@@ -403,119 +394,127 @@
     send_v, recv_v, send_s, recv_s, send_a, recv_a, send_r, recv_r, send_q, recv_q, send_o, recv_o,
 ):
     me_k, me_t = lax.axis_index("kv"), lax.axis_index("tp")
+    mine = me_t * n_kv + me_k
     heads, _, _ = part_ref.shape
     v_dim = wv_ref.shape[1]
-    kv_peers = [lax.rem(me_k + d, n_kv) for d in range(n_kv)]
-    tp_peers = [lax.rem(me_t + d, n_tp) for d in range(n_tp)]
+    pieces, _, each, _ = vals.shape
+    kv_peers = [flip(me_k, d) for d in range(n_kv)]
+    tp_peers = [flip(me_t, d) for d in range(n_tp)]
     barrier = pltpu.get_barrier_semaphore()
-    for dk in range(n_kv):
-        for dt in range(n_tp):
-            if dk or dt:
-                pl.semaphore_signal(
-                    barrier, inc=1,
-                    device_id={"kv": kv_peers[dk], "tp": tp_peers[dt]}, device_id_type=MESH,
-                )
+    everyone = [(dk, dt) for dt in range(n_tp) for dk in range(n_kv) if dk or dt]
+    for dk, dt in everyone:
+        pl.semaphore_signal(
+            barrier, inc=1,
+            device_id={"kv": kv_peers[dk], "tp": tp_peers[dt]}, device_id_type=MESH,
+        )
     sends = []
 
-    each = vals.shape[1]
-    line = lax.broadcasted_iota(jnp.int32, (16, LANES), 0)
-    lane = lax.broadcasted_iota(jnp.int32, (16, LANES), 1)
+    line, lane = iota((8, LANES), 0), iota((8, LANES), 1)
     tops = (line < heads) & (lane == line)
-    counts = (line >= 8) & (line < 8 + heads) & (lane == line - 8 + heads)
+    counts = (line >= 4) & (line < 4 + heads) & (lane == line - 4 + heads)
     pick = jnp.where(tops | counts, 1.0, 0.0)
     values = jnp.concatenate([dot_nt(part_ref[h], wv_ref[h]) for h in range(heads)], axis=1)
-    for j in range(n_kv):
-        vals[j] = values[j * each : (j + 1) * each].astype(jnp.bfloat16)
-        stat[j] = dot_nt(pick, stats_ref[j * each : (j + 1) * each, :], HIGHEST)
+    for c in range(pieces):
+        for j in range(n_kv):
+            lines = slice((j * pieces + c) * each, (j * pieces + c + 1) * each)
+            vals[c, j] = values[lines].astype(jnp.bfloat16)
+            stat[c, j] = dot_nt(pick, stats_ref[lines, :], HIGHEST)
     pl.semaphore_wait(barrier, n_kv * n_tp - 1)
 
-    def exchange(axis, peers, src_of, dst, own, send_sem, recv_sem):
-        for d in range(1, len(peers)):
+    def exchange(c, axis, peers, src_of, dst, own, send_sem, recv_sem):
+        for d in reversed(range(1, len(peers))):
             copy = remote(
-                src_of(peers[d]), dst.at[own], send_sem.at[d], recv_sem.at[own], {axis: peers[d]}
+                src_of(peers[d]), dst.at[c, own], send_sem.at[c, d], recv_sem.at[c, own],
+                {axis: peers[d]},
             )
             copy.start()
             sends.append(copy)
 
-    def arrived(axis, peers, d, src_of, dst, send_sem, recv_sem):
+    def arrived(c, axis, peers, d, dst, send_sem, recv_sem):
+        here = dst.at[c, peers[d]]
         remote(
-            src_of(peers[d]), dst.at[peers[d]], send_sem.at[d], recv_sem.at[peers[d]],
-            {axis: peers[d]},
+            here, here, send_sem.at[c, d], recv_sem.at[c, peers[d]], {axis: peers[d]}
         ).wait_recv()
 
-    exchange("kv", kv_peers, lambda p: stat.at[p], got_stat, me_k, send_s, recv_s)
-    exchange("kv", kv_peers, lambda p: vals.at[p], got_vals, me_k, send_v, recv_v)
-    for d in range(1, n_kv):
-        arrived("kv", kv_peers, d, lambda p: stat.at[p], got_stat, send_s, recv_s)
-    all_stats = [stat[me_k]] + [got_stat[p] for p in kv_peers[1:]]
-    largest = all_stats[0][:8]
-    for one in all_stats[1:]:
-        largest = jnp.maximum(largest, one[:8])
-    shares = jnp.concatenate([one[8:] * jnp.exp(one[:8] - largest) for one in all_stats], axis=0)
-    turn_eye = lax.broadcasted_iota(jnp.int32, (each, each), 0) == lax.broadcasted_iota(
-        jnp.int32, (each, each), 1
-    )
-    shares = dot_nt(turn_eye.astype(jnp.float32), shares, HIGHEST)
-    wide = lax.broadcasted_iota(jnp.int32, (each, heads * v_dim), 1)
-
-    def spread(d):
-        out = shares[:, 8 * d : 8 * d + 1]
-        for h in range(1, heads):
-            out = jnp.where(wide >= h * v_dim, shares[:, 8 * d + h : 8 * d + h + 1], out)
-        return jnp.broadcast_to(out, wide.shape)
-
-    summed = None
-    for d in range(n_kv):
-        share = spread(d)
-        if d:
-            arrived("kv", kv_peers, d, lambda p: vals.at[p], got_vals, send_v, recv_v)
-        block = got_vals[kv_peers[d]] if d else vals[me_k]
-        term = share * block.astype(jnp.float32)
-        summed = term if summed is None else summed + term
-        weight = share if d == 0 else weight + share
-    attended[me_k] = (summed / weight).astype(jnp.bfloat16)
-    exchange("kv", kv_peers, lambda p: attended.at[me_k], attended, me_k, send_a, recv_a)
-    for d in range(1, n_kv):
-        arrived("kv", kv_peers, d, lambda p: attended.at[p], attended, send_a, recv_a)
-
-    lines = jnp.concatenate([attended[j].astype(jnp.float32) for j in range(n_kv)], axis=0)
-    lines = dot(lines.astype(jnp.bfloat16), w_out_ref[...])
-    share_rows, cols = raw.shape[1:]
-    for t in range(n_tp):
-        raw[t] = lines[t * share_rows : (t + 1) * share_rows].astype(jnp.bfloat16)
-    exchange("tp", tp_peers, lambda p: raw.at[p], got_raw, me_t, send_r, recv_r)
-    mixed = raw[me_t].astype(jnp.float32)
-    for d in range(1, n_tp):
-        arrived("tp", tp_peers, d, lambda p: raw.at[p], got_raw, send_r, recv_r)
-        mixed = mixed + got_raw[tp_peers[d]].astype(jnp.float32)
-    result[me_t] = mixed.astype(jnp.bfloat16)
-    exchange("tp", tp_peers, lambda p: result.at[me_t], result, me_t, send_o, recv_o)
-    mine = me_t * n_kv + me_k
-    sums[mine] = dot_nt(jnp.ones((8, cols), jnp.float32), mixed * mixed, HIGHEST)
-    everyone = [(dk, dt) for dt in range(n_tp) for dk in range(n_kv) if dk or dt]
-    for n, (dk, dt) in enumerate(everyone):
-        copy = remote(
-            sums.at[mine], sums.at[mine], send_q.at[n], recv_q.at[mine],
-            {"kv": kv_peers[dk], "tp": tp_peers[dt]},
+    for c in range(pieces):
+        exchange(c, "kv", kv_peers, lambda p: stat.at[c, p], got_stat, me_k, send_s, recv_s)
+        exchange(c, "kv", kv_peers, lambda p: vals.at[c, p], got_vals, me_k, send_v, recv_v)
+
+    eye = iota((each, each), 0) == iota((each, each), 1)
+    wide = iota((each, heads * v_dim), 1)
+    for c in range(pieces):
+        for d in range(1, n_kv):
+            arrived(c, "kv", kv_peers, d, got_stat, send_s, recv_s)
+        all_stats = [stat[c, me_k]] + [got_stat[c, p] for p in kv_peers[1:]]
+        largest = all_stats[0]
+        for one in all_stats[1:]:
+            largest = jnp.maximum(largest, one)
+        largest = largest[:4]
+        shares = [one[4:] * jnp.exp(one[:4] - largest) for one in all_stats]
+        shares = dot_nt(eye.astype(jnp.float32), jnp.concatenate(shares, axis=0), HIGHEST)
+        summed = None
+        for d in range(n_kv):
+            share = shares[:, 4 * d : 4 * d + 1]
+            for h in range(1, heads):
+                share = jnp.where(wide >= h * v_dim, shares[:, 4 * d + h : 4 * d + h + 1], share)
+            share = jnp.broadcast_to(share, wide.shape)
+            if d:
+                arrived(c, "kv", kv_peers, d, got_vals, send_v, recv_v)
+            block = got_vals[c, kv_peers[d]] if d else vals[c, me_k]
+            term = share * block.astype(jnp.float32)
+            summed = term if summed is None else summed + term
+            weight = share if d == 0 else weight + share
+        attended[c, me_k] = (summed / weight).astype(jnp.bfloat16)
+        exchange(
+            c, "kv", kv_peers, lambda p: attended.at[c, me_k], attended, me_k, send_a, recv_a
         )
-        copy.start()
-        sends.append(copy)
-    for n, (dk, dt) in enumerate(everyone):
-        source = tp_peers[dt] * n_kv + kv_peers[dk]
-        remote(
-            sums.at[source], sums.at[source], send_q.at[n], recv_q.at[source],
-            {"kv": kv_peers[dk], "tp": tp_peers[dt]},
-        ).wait_recv()
+
+    share_rows, cols = raw.shape[2:]
+    for c in range(pieces):
+        for d in range(1, n_kv):
+            arrived(c, "kv", kv_peers, d, attended, send_a, recv_a)
+        lines = [attended[c, j].astype(jnp.float32) for j in range(n_kv)]
+        lines = dot(jnp.concatenate(lines, axis=0).astype(jnp.bfloat16), w_out_ref[...])
+        for t in range(n_tp):
+            raw[c, t] = lines[t * share_rows : (t + 1) * share_rows].astype(jnp.bfloat16)
+        exchange(c, "tp", tp_peers, lambda p: raw.at[c, p], got_raw, me_t, send_r, recv_r)
+
+    for c in range(pieces):
+        mixed = raw[c, me_t].astype(jnp.float32)
+        for d in range(1, n_tp):
+            arrived(c, "tp", tp_peers, d, got_raw, send_r, recv_r)
+            mixed = mixed + got_raw[c, tp_peers[d]].astype(jnp.float32)
+        result[c, me_t] = mixed.astype(jnp.bfloat16)
+        sums[c, mine] = dot_nt(jnp.ones((8, cols), jnp.float32), mixed * mixed, HIGHEST)
+        for n, (dk, dt) in reversed(list(enumerate(everyone))):
+            copy = remote(
+                sums.at[c, mine], sums.at[c, mine], send_q.at[c, n], recv_q.at[c, mine],
+                {"kv": kv_peers[dk], "tp": tp_peers[dt]},
+            )
+            copy.start()
+            sends.append(copy)
+        exchange(c, "tp", tp_peers, lambda p: result.at[c, me_t], result, me_t, send_o, recv_o)
+
     eye = iota((share_rows, share_rows), 0) == iota((share_rows, share_rows), 1)
-    for d in range(1, n_tp):
-        arrived("tp", tp_peers, d, lambda p: result.at[p], result, send_o, recv_o)
-    for t in range(n_tp):
-        square = sums[t * n_kv]
-        for j in range(1, n_kv):
-            square = square + sums[t * n_kv + j]
-        norm = lax.rsqrt(square / (cols * n_kv) + epsilon)
-        column = jnp.sum(jnp.where(eye, norm[:1], 0.0), axis=1, keepdims=True)
-        out_ref[t] = (result[t].astype(jnp.float32) * column * gain_ref[...]).astype(jnp.bfloat16)
+    for c in range(pieces):
+        for d in range(1, n_tp):
+            arrived(c, "tp", tp_peers, d, result, send_o, recv_o)
+        for n, (dk, dt) in enumerate(everyone):
+            source = tp_peers[dt] * n_kv + kv_peers[dk]
+            here = sums.at[c, source]
+            remote(
+                here, here, send_q.at[c, n], recv_q.at[c, source],
+                {"kv": kv_peers[dk], "tp": tp_peers[dt]},
+            ).wait_recv()
+        for t in range(n_tp):
+            square = sums[c, t * n_kv]
+            for j in range(1, n_kv):
+                square = square + sums[c, t * n_kv + j]
+            norm = lax.rsqrt(square / (cols * n_kv) + epsilon)
+            column = jnp.sum(jnp.where(eye, norm[:1], 0.0), axis=1, keepdims=True)
+            rows = result[c, t].astype(jnp.float32) * column * gain_ref[...]
+            for o in range(share_rows // each):
+                out_ref[t, o, c] = rows[o * each : (o + 1) * each].astype(jnp.bfloat16)
     for copy in sends:
         copy.wait_send()
 
@@ -628,7 +627,8 @@
         scratch_shapes=[
             pltpu.VMEM((seqs, heads * props, kv_rank), bf16),
             pltpu.VMEM((seqs, heads * props, turn_dim), bf16),
-            pltpu.VMEM((group, props, span), f32),
+            pltpu.VMEM((seqs, props, span), f32),
+            pltpu.VMEM((group, span, kv_rank), bf16),
             dma((seqs,)),
         ],
         input_output_aliases={6: 3},
@@ -640,26 +640,27 @@
     )
 
     wv = lax.dynamic_slice_in_dim(w_value.transpose(0, 2, 1), me_t * heads, heads, 0)
-    per_kv, per_tp = rows // n_kv, rows // n_tp
+    per_kv, share = rows // n_kv, n_kv // n_tp
+    pieces = 1
+    lot = per_kv // pieces
     mixed = pl.pallas_call(
         functools.partial(project_kernel, n_kv, n_tp),
         name="project",
-        out_shape=jax.ShapeDtypeStruct((n_tp, per_tp, cols), bf16),
+        out_shape=jax.ShapeDtypeStruct((n_tp, share, pieces, lot, cols), bf16),
         in_specs=[VMEM] * 5,
         out_specs=VMEM,
         scratch_shapes=[
-            pltpu.VMEM((n_kv, per_kv, heads * v_dim), bf16),
-            pltpu.VMEM((n_kv, 16, per_kv), f32),
-            pltpu.VMEM((n_kv, per_kv, heads * v_dim), bf16),
-            pltpu.VMEM((n_kv, 16, per_kv), f32),
-            pltpu.VMEM((n_kv, per_kv, heads * v_dim), bf16),
-            pltpu.VMEM((n_tp, per_tp, cols), bf16),
-            pltpu.VMEM((n_tp, per_tp, cols), bf16),
-            pltpu.VMEM((n_dev, 8, per_tp), f32),
-            pltpu.VMEM((n_tp, per_tp, cols), bf16),
-            dma((n_kv,)), dma((n_kv,)), dma((n_kv,)), dma((n_kv,)), dma((n_kv,)), dma((n_kv,)),
-            dma((n_tp,)), dma((n_tp,)), dma((n_dev,)), dma((n_dev,)), dma((n_tp,)), dma((n_tp,)),
-        ],
+            pltpu.VMEM((pieces, n_kv, lot, heads * v_dim), bf16),
+            pltpu.VMEM((pieces, n_kv, 8, lot), f32),
+            pltpu.VMEM((pieces, n_kv, lot, heads * v_dim), bf16),
+            pltpu.VMEM((pieces, n_kv, 8, lot), f32),
+            pltpu.VMEM((pieces, n_kv, lot, heads * v_dim), bf16),
+            pltpu.VMEM((pieces, n_tp, share * lot, cols), bf16),
+            pltpu.VMEM((pieces, n_tp, share * lot, cols), bf16),
+            pltpu.VMEM((pieces, n_dev, 8, share * lot), f32),
+            pltpu.VMEM((pieces, n_tp, share * lot, cols), bf16),
+        ]
+        + [dma((pieces, n)) for n in (n_kv,) * 6 + (n_tp,) * 2 + (n_dev,) * 2 + (n_tp,) * 2],
         compiler_params=pltpu.CompilerParams(
             collective_id=1, has_side_effects=True, vmem_limit_bytes=32 * 1024 * 1024
         ),

time: 87 us -> 79.2 us (0.910); the launches traced: 85.9 us -> 79 us
  Pallas kernels: 84.4 us -> 77.5 us
    pallas_call x1, Pallas kernels: 21.1 us -> 16.1 us  [local(): pl.pallas_call(functools.partial(attend_kernel, group), name='attend', ou...]
    pallas_call x1, Pallas kernels: 29.7 us -> 27.7 us  [local(): pl.pallas_call(functools.partial(project_kernel, n_kv, n_tp), name='proje...]
where the time goes in v2:
time: 79.2 us; the launch traced here: 79 us
  Pallas kernels  77.5 us (98%)
    pallas_call x1, Pallas kernels, local(): pl.pallas_call(functools.partial(compress_kernel, n_kv, n_tp, few), name=...  33.7 us
    pallas_call x1, Pallas kernels, local(): pl.pallas_call(functools.partial(project_kernel, n_kv, n_tp), name='proje...  27.7 us
    pallas_call x1, Pallas kernels, local(): pl.pallas_call(functools.partial(attend_kernel, group), name='attend', ou...  16.1 us

profile of v2, /device:TPU:0, one launch (start us, length us, event | category | flops | bytes accessed | tf_op | source)
XLA Modules:
  0.0 79.0 jit_solution(6869523182814401479)
XLA Ops:
  0.6 0.0 copy-start
  0.6 0.0 copy-start.2
  0.7 0.0 copy-start.3
  0.7 0.0 copy-start.4
  0.7 0.0 copy-start.1
  0.7 33.7 %compress.1 = (bf16[16,24,512]{2,1,0:T(8,128)(2,1)S(1)}, bf16[16,24,384]{2,1,0:T(8,128)(2,1)S(1)}, f32[392,128]{1,0:T(8,128)S(1)}, bf16[4,288,512]{2,1,0:T(8,128)(2,1)S(1)}, bf16[24,288,2048]{2,1,0:T(8,128)(2,1)S(1)}) custom-call(bf16[64,384]{1,0:T(8,128)(2,1)} %bitcast.17, bf16[64,512]{1,0:T(8,128)(2,1)} %wq_hbm.1, bf16[64,288]{1,0:T(8,128)(2,1)} %wk_hbm.1, ...), custom_call_target="tpu_custom_call" | custom-call | tf_op jit(solution)/shard_map/compress/pallas_call | solution.py:567
  34.4 0.0 copy-done.2
  34.4 0.0 copy-done.3
  34.4 16.1 %attend.1 = (bf16[24,288,2048]{2,1,0:T(8,128)(2,1)}, bf16[4,384,256]{2,1,0:T(8,128)(2,1)S(1)}, f32[384,128]{1,0:T(8,128)S(1)}, bf16[24,288,2048]{2,1,0:T(8,128)(2,1)S(1)}) custom-call(s32[24]{0:T(128)S(1)} %copy-done.2, s32[24]{0:T(128)S(1)} %copy-done.3, bf16[384,512]{1,0:T(8,128)(2,1)S(1)} %bitcast.12, ...), custom_call_target="tpu_custom_call", output_to_operand_aliasing={{3}: (6, {})} | custom-call | tf_op jit(solution)/shard_map/attend/pallas_call | solution.py:616
  50.6 0.0 copy-done
  50.6 0.0 copy-done.4
  50.6 0.0 copy-done.1
  50.6 27.7 %project.1 = bf16[4,2,1,48,256]{4,3,2,1,0:T(8,128)(2,1)S(1)} custom-call(bf16[4,384,256]{2,1,0:T(8,128)(2,1)S(1)} %get-tuple-element.15.part_ref, f32[384,128]{1,0:T(8,128)S(1)} %get-tuple-element.16.stats_ref, bf16[4,64,256]{2,1,0:T(8,128)(2,1)S(1)} %dynamic-slice_bitcast_fusion.wv_ref, bf16[256,256]{1,0:T(8,128)(2,1)S(1)} %copy-done.1, f32[1,256]{1,0:T(1,128)S(1)} %bitcast.14), custom_call_target="tpu_custom_call" | custom-call | tf_op jit(solution)/shard_map/project/pallas_call | solution.py:646
  78.3 0.7 copy.19
  (3 shorter events, 0.0 us)
Async XLA Ops:
  0.6 49.9 %copy-start = (bf16[16,256,64]{1,2,0:T(8,128)(2,1)S(1)}, bf16[16,256,64]{1,2,0:T(8,128)(2,1)}, u32[]{:S(2)}) copy-start(bf16[16,256,64]{1,2,0:T(8,128)(2,1)} %param.25) | copy-start | bytes 1572868
  0.6 33.7 %copy-start.2 = (s32[24]{0:T(128)S(1)}, s32[24]{0:T(128)}, u32[]{:S(2)}) copy-start(s32[24]{0:T(128)} %lengths_ref.1) | copy-start | bytes 292
  0.7 33.7 %copy-start.3 = (s32[24]{0:T(128)S(1)}, s32[24]{0:T(128)}, u32[]{:S(2)}) copy-start(s32[24]{0:T(128)} %accepted_ref.1) | copy-start | bytes 292
  0.7 49.9 %copy-start.4 = (bf16[256]{0:T(256)(128)(2,1)S(1)}, bf16[256]{0:T(256)(128)(2,1)}, u32[]{:S(2)}) copy-start(bf16[256]{0:T(256)(128)(2,1)} %param.27) | copy-start | bytes 1540
  0.7 49.9 %copy-start.1 = (bf16[256,256]{1,0:T(8,128)(2,1)S(1)}, bf16[256,256]{1,0:T(8,128)(2,1)}, u32[]{:S(2)}) copy-start(bf16[256,256]{1,0:T(8,128)(2,1)} %w_out_ref.1) | copy-start | bytes 393220

commit v3 on v2

--- a/solution.py
+++ b/solution.py
@@ -92,22 +92,19 @@
     x_hbm, wq_hbm, wk_hbm, gain_x_hbm, gain_q_hbm, gain_k_hbm, parents_hbm,
     lengths_hbm, accepted_hbm, freq_ref, expand_hbm, cache_hbm,
     q_all, k_all, table_ref, expand_ref, held_ref,
-    x_own, wq_own, wk_raw, gain_x, gain_q, gain_k, parents_ref, lengths, accepted, wk_own, x_msg, got_x, got_wq, got_wk, part, got_part, sq_all,
+    x_own, wq_own, wk_raw, gain_x, gain_q, gain_k, parents_ref, lengths, accepted, wk_own, x_msg, got_x, got_wq, got_wk, part_q, got_q, part_k, got_k, sq_tp, sq_kv,
     fetch_s, fetch_c,
-    send_x, recv_x, send_w, recv_w, send_s, recv_s, send_p, recv_p,
+    send_x, recv_x, send_w, recv_w, send_s, recv_s, send_z, recv_z, send_p, recv_p,
     send_a, send_y, send_b, recv_q, recv_k,
 ):
     me_k, me_t = lax.axis_index("kv"), lax.axis_index("tp")
     n_y = n_tp // 2
     me_y, core = lax.div(me_t, 2), lax.rem(me_t, 2)
-    mine = me_t * n_kv + me_k
     barrier = pltpu.get_barrier_semaphore()
-    everyone = [(dk, dt) for dk in range(n_kv) for dt in range(n_tp) if dk or dt]
-    for dk, dt in everyone:
-        pl.semaphore_signal(
-            barrier, inc=1,
-            device_id={"kv": flip(me_k, dk), "tp": flip(me_t, dt)}, device_id_type=MESH,
-        )
+    partners = [{"kv": flip(me_k, d)} for d in range(1, n_kv)]
+    partners += [{"tp": flip(me_t, d)} for d in range(1, n_tp)]
+    for partner in partners:
+        pl.semaphore_signal(barrier, inc=1, device_id=partner, device_id_type=MESH)
     small = [
         pltpu.make_async_copy(src, dst, fetch_s.at[n])
         for n, (src, dst) in enumerate(
@@ -130,12 +127,12 @@
     features, rows = x_own.shape
     q_rank, kv_rank = gain_q.shape[-1], gain_k.shape[-1]
     whole, wide = wk_raw.shape[1], wk_own.shape[1]
-    each, half = part.shape[1], x_msg.shape[1]
+    each, half = part_q.shape[1], x_msg.shape[1]
     raw = x_own[...].astype(jnp.float32)
     squares = jnp.sum(raw * raw, axis=0, keepdims=True)
-    sq_all[mine] = jnp.zeros_like(sq_all[0])
+    sq_tp[me_t] = jnp.zeros_like(sq_tp[0])
     for n in range(rows // LANES):
-        sq_all[mine, n : n + 1, :] = squares[:, n * LANES : (n + 1) * LANES]
+        sq_tp[me_t, n : n + 1, :] = squares[:, n * LANES : (n + 1) * LANES]
     scaled = raw.T * gain_x[...].astype(jnp.float32)[None]
     for y in range(n_y):
         for n in range(2):
@@ -152,7 +149,7 @@
             x_msg[y, :, n * features : (n + 1) * features] = value
     wk_own[...] = jnp.zeros_like(wk_own)
     wk_own[:, :whole] = wk_raw[...]
-    pl.semaphore_wait(barrier, n_kv * n_tp - 1)
+    pl.semaphore_wait(barrier, len(partners))
 
     def role(c):
         sends = []
@@ -162,7 +159,8 @@
             copy.start()
             sends.append(copy)
 
-        w_own, got_w, width = (wq_own, got_wq, q_rank) if c == 0 else (wk_own, got_wk, wide)
+        w_own, got_w = (wq_own, got_wq) if c == 0 else (wk_own, got_wk)
+        part, got_part = (part_q, got_q) if c == 0 else (part_k, got_k)
         for dt in reversed(range(1, n_tp)):
             peer = flip(me_t, dt)
             theirs, land = (wq_own, got_wq) if (c ^ dt) % 2 == 0 else (wk_own, got_wk)
@@ -171,11 +169,7 @@
                 x_msg.at[lax.div(peer, 2)], got_x.at[me_t], send_x.at[dt], recv_x.at[me_t],
                 {"tp": peer},
             )
-        for n, (dk, dt) in enumerate(everyone):
-            start(
-                sq_all.at[mine], sq_all.at[mine], send_s.at[n], recv_s.at[mine],
-                {"kv": flip(me_k, dk), "tp": flip(me_t, dt)},
-            )
+            start(sq_tp.at[me_t], sq_tp.at[me_t], send_s.at[dt], recv_s.at[me_t], {"tp": peer})
         for copy in big:
             copy.start()
         table_ref[:rows] = row_table(
@@ -188,6 +182,13 @@
             remote(
                 x_msg.at[0], got_x.at[peer], send_x.at[dt], recv_x.at[peer], {"tp": peer}
             ).wait_recv()
+            remote(
+                sq_tp.at[peer], sq_tp.at[peer], send_s.at[dt], recv_s.at[peer], {"tp": peer}
+            ).wait_recv()
+        square = sq_tp[0]
+        for t in range(1, n_tp):
+            square = square + sq_tp[t]
+        sq_kv[me_k] = square
         terms = [(x_msg[me_y], w_own[...])]
         for dt in range(1, n_tp):
             peer = flip(me_t, dt)
@@ -198,26 +199,28 @@
                 term = dot(x[:, n * features : (n + 1) * features], w)
                 total = term if total is None else total + term
             for j in range(n_kv // 2):
-                part[n * (n_kv // 2) + j, :, :width] = total[j * each : (j + 1) * each]
-
-        cut = pl.ds(0, width)
+                part[n * (n_kv // 2) + j] = total[j * each : (j + 1) * each].astype(part.dtype)
+
+        used = pl.ds(0, rows // LANES)
+        for dk in reversed(range(1, n_kv)):
+            peer = flip(me_k, dk)
+            mine = sq_kv.at[me_k, used]
+            start(mine, mine, send_z.at[dk], recv_z.at[me_k], {"kv": peer})
         for dk in reversed(range(1, n_kv)):
             peer = flip(me_k, dk)
             start(
-                part.at[peer, :, cut], got_part.at[me_k, :, cut], send_p.at[dk],
+                part.at[peer], got_part.at[me_k], send_p.at[dk],
                 recv_p.at[me_k], {"kv": peer},
             )
         block = me_y * n_kv + me_k
         first = block * few
-        for n, (dk, dt) in enumerate(everyone):
-            source = flip(me_t, dt) * n_kv + flip(me_k, dk)
-            remote(
-                sq_all.at[source], sq_all.at[source], send_s.at[n], recv_s.at[source],
-                {"kv": flip(me_k, dk), "tp": flip(me_t, dt)},
-            ).wait_recv()
-        square = sq_all[0]
-        for n in range(1, n_kv * n_tp):
-            square = square + sq_all[n]
+        for dk in range(1, n_kv):
+            peer = flip(me_k, dk)
+            here = sq_kv.at[peer, used]
+            remote(here, here, send_z.at[dk], recv_z.at[peer], {"kv": peer}).wait_recv()
+        square = sq_kv[0, : rows // LANES]
+        for k in range(1, n_kv):
+            square = square + sq_kv[k, : rows // LANES]
         column = jnp.zeros((each, 1), jnp.float32)
         for n in range(rows // LANES):
             here = iota((each, LANES), 1) + n * LANES == iota((each, LANES), 0) + first
@@ -225,14 +228,14 @@
                 jnp.where(here, square[n : n + 1], 0.0), axis=1, keepdims=True
             )
         inverse = lax.rsqrt(column / (n_kv * n_tp * features) + epsilon)
-        summed = part[me_k, :, :width]
+        summed = part[me_k].astype(jnp.float32)
         for dk in range(1, n_kv):
             peer = flip(me_k, dk)
             remote(
-                part.at[peer, :, cut], got_part.at[peer, :, cut], send_p.at[dk],
+                part.at[peer], got_part.at[peer], send_p.at[dk],
                 recv_p.at[peer], {"kv": peer},
             ).wait_recv()
-            summed = summed + got_part[peer, :, :width]
+            summed = summed + got_part[peer].astype(jnp.float32)
         if c == 0:
             query = summed * inverse
             query = query * root_mean(query, q_rank) * gain_q[...].astype(jnp.float32)[None]
@@ -591,12 +594,15 @@
             pltpu.VMEM((n_tp, n_kv * each // 2, 2 * features), bf16),
             pltpu.VMEM((n_tp, features, q_rank), bf16),
             pltpu.VMEM((n_tp, features, wide), bf16),
-            pltpu.VMEM((n_kv, each, max(q_rank, wide)), f32),
-            pltpu.VMEM((n_kv, each, max(q_rank, wide)), f32),
-            pltpu.VMEM((n_dev, 8, LANES), f32),
+            pltpu.VMEM((n_kv, each, q_rank), f32),
+            pltpu.VMEM((n_kv, each, q_rank), f32),
+            pltpu.VMEM((n_kv, each, wide), bf16),
+            pltpu.VMEM((n_kv, each, wide), bf16),
+            pltpu.VMEM((n_tp, 8, LANES), f32),
+            pltpu.VMEM((n_kv, 8, LANES), f32),
             dma((10,)), dma((seqs,)),
             dma((n_tp,)), dma((n_tp,)), dma((n_tp,)), dma((n_tp,)),
-            dma((n_dev,)), dma((n_dev,)), dma((n_kv,)), dma((n_kv,)),
+            dma((n_tp,)), dma((n_tp,)), dma((n_kv,)), dma((n_kv,)), dma((n_kv,)), dma((n_kv,)),
             dma((n_kv,)), dma((blocks,)), dma((blocks,)), dma((blocks,)), dma((blocks,)),
         ],
         compiler_params=pltpu.CompilerParams(

time: 79.2 us -> 75.6 us (0.955); the launches traced: 79 us -> 76.2 us
  Pallas kernels: 77.5 us -> 74.7 us
    pallas_call x1, Pallas kernels: 33.7 us -> 30.1 us  [local(): pl.pallas_call(functools.partial(compress_kernel, n_kv, n_tp, few), name=...]
    pallas_call x1, Pallas kernels: 27.7 us -> 28.5 us  [local(): pl.pallas_call(functools.partial(project_kernel, n_kv, n_tp), name='proje...]
where the time goes in v3:
time: 75.6 us; the launch traced here: 76.2 us
  Pallas kernels  74.7 us (99%)
    pallas_call x1, Pallas kernels, local(): pl.pallas_call(functools.partial(compress_kernel, n_kv, n_tp, few), name=...  30.1 us
    pallas_call x1, Pallas kernels, local(): pl.pallas_call(functools.partial(project_kernel, n_kv, n_tp), name='proje...  28.5 us
    pallas_call x1, Pallas kernels, local(): pl.pallas_call(functools.partial(attend_kernel, group), name='attend', ou...  16.1 us

profile of v3, /device:TPU:0, one launch (start us, length us, event | category | flops | bytes accessed | tf_op | source)
XLA Modules:
  0.0 76.2 jit_solution(1459890661668435249)
XLA Ops:
  0.6 0.0 copy-start
  0.6 0.0 copy-start.2
  0.7 0.0 copy-start.3
  0.7 0.0 copy-start.4
  0.7 0.0 copy-start.1
  0.7 30.1 %compress.1 = (bf16[16,24,512]{2,1,0:T(8,128)(2,1)S(1)}, bf16[16,24,384]{2,1,0:T(8,128)(2,1)S(1)}, f32[392,128]{1,0:T(8,128)S(1)}, bf16[4,288,512]{2,1,0:T(8,128)(2,1)S(1)}, bf16[24,288,2048]{2,1,0:T(8,128)(2,1)S(1)}) custom-call(bf16[64,384]{1,0:T(8,128)(2,1)} %bitcast.17, bf16[64,512]{1,0:T(8,128)(2,1)} %wq_hbm.1, bf16[64,288]{1,0:T(8,128)(2,1)} %wk_hbm.1, ...), custom_call_target="tpu_custom_call" | custom-call | tf_op jit(solution)/shard_map/compress/pallas_call | solution.py:570
  30.8 0.0 copy-done.2
  30.8 0.0 copy-done.3
  30.8 16.1 %attend.1 = (bf16[24,288,2048]{2,1,0:T(8,128)(2,1)}, bf16[4,384,256]{2,1,0:T(8,128)(2,1)S(1)}, f32[384,128]{1,0:T(8,128)S(1)}, bf16[24,288,2048]{2,1,0:T(8,128)(2,1)S(1)}) custom-call(s32[24]{0:T(128)S(1)} %copy-done.2, s32[24]{0:T(128)S(1)} %copy-done.3, bf16[384,512]{1,0:T(8,128)(2,1)S(1)} %bitcast.12, ...), custom_call_target="tpu_custom_call", output_to_operand_aliasing={{3}: (6, {})} | custom-call | tf_op jit(solution)/shard_map/attend/pallas_call | solution.py:622
  47.0 0.0 copy-done
  47.0 0.0 copy-done.4
  47.0 0.0 copy-done.1
  47.1 28.5 %project.1 = bf16[4,2,1,48,256]{4,3,2,1,0:T(8,128)(2,1)S(1)} custom-call(bf16[4,384,256]{2,1,0:T(8,128)(2,1)S(1)} %get-tuple-element.15.part_ref, f32[384,128]{1,0:T(8,128)S(1)} %get-tuple-element.16.stats_ref, bf16[4,64,256]{2,1,0:T(8,128)(2,1)S(1)} %dynamic-slice_bitcast_fusion.wv_ref, bf16[256,256]{1,0:T(8,128)(2,1)S(1)} %copy-done.1, f32[1,256]{1,0:T(1,128)S(1)} %bitcast.14), custom_call_target="tpu_custom_call" | custom-call | tf_op jit(solution)/shard_map/project/pallas_call | solution.py:652
  75.6 0.7 copy.19
  (3 shorter events, 0.0 us)
Async XLA Ops:
  0.6 46.4 %copy-start = (bf16[16,256,64]{1,2,0:T(8,128)(2,1)S(1)}, bf16[16,256,64]{1,2,0:T(8,128)(2,1)}, u32[]{:S(2)}) copy-start(bf16[16,256,64]{1,2,0:T(8,128)(2,1)} %param.25) | copy-start | bytes 1572868
  0.6 30.2 %copy-start.2 = (s32[24]{0:T(128)S(1)}, s32[24]{0:T(128)}, u32[]{:S(2)}) copy-start(s32[24]{0:T(128)} %lengths_ref.1) | copy-start | bytes 292
  0.7 30.2 %copy-start.3 = (s32[24]{0:T(128)S(1)}, s32[24]{0:T(128)}, u32[]{:S(2)}) copy-start(s32[24]{0:T(128)} %accepted_ref.1) | copy-start | bytes 292
  0.7 46.3 %copy-start.4 = (bf16[256]{0:T(256)(128)(2,1)S(1)}, bf16[256]{0:T(256)(128)(2,1)}, u32[]{:S(2)}) copy-start(bf16[256]{0:T(256)(128)(2,1)} %param.27) | copy-start | bytes 1540
  0.7 46.4 %copy-start.1 = (bf16[256,256]{1,0:T(8,128)(2,1)S(1)}, bf16[256,256]{1,0:T(8,128)(2,1)}, u32[]{:S(2)}) copy-start(bf16[256,256]{1,0:T(8,128)(2,1)} %w_out_ref.1) | copy-start | bytes 393220
